TPU v7x, 32 devices: a whole 2x2x4 slice. The times are simulated.
32 devices in a mesh: sp: 4 (over y, x), tp: 8 (over z, core).
Axes of the slice: x: 2, y: 2, z: 4, core: 2. Of those that a mesh axis runs over, the one named last changes fastest.
Arguments:
- residual_in: bfloat16 [1024, 4096], P(('sp', 'tp')), may hold values from -6 to 6
- queries: bfloat16 [1024, 2048], P('sp', 'tp'), may hold values from -6 to 6
- keys: bfloat16 [1024, 2048], P('sp', 'tp'), may hold values from -6 to 6
- values: bfloat16 [1024, 2048], P('sp', 'tp'), may hold values from -6 to 6
- break_offset: bfloat16 [1024, 32], P('sp', 'tp'), may hold values from -14 to 1
- doc_ids: int32 [1024], P('sp'), may hold values from 0 to 2, never falling along the last dimension, each value on 1 to 640 neighbouring positions
- out_weight: bfloat16 [2048, 4096], P('tp'), may hold values from -0.125 to 0.125
- norm_gain: float32 [4096], replicated, may hold values from 0.1 to 1.9
- group_router: bfloat16 [4096, 2], replicated, may hold values from -0.1875 to 0.1875
- expert_router: bfloat16 [4096, 4], replicated, may hold values from -0.1875 to 0.1875
- expert_ids: int32 [1024, 2], P('sp'), may hold values from 0 to 3, as said below
- gate_weight: bfloat16 [4, 4096, 4096], P('sp', None, 'tp'), may hold values from -0.09375 to 0.09375
- up_weight: bfloat16 [4, 4096, 4096], P('sp', None, 'tp'), may hold values from -0.09375 to 0.09375
- down_weight: bfloat16 [4, 4096, 4096], P('sp', 'tp'), may hold values from -0.09375 to 0.09375
Outputs:
- layer_out: bfloat16 [1024, 4096], P(('sp', 'tp'))
Inputs may be any that keep to these rules, and one draw needn't show every extreme that they name: `doc_ids`: document numbers never fall along the positions; one document covers exactly 640 positions. `expert_ids`: the two experts of a position differ and lie in one group of 2 consecutive numbers; in each aligned block of 32 positions every expert is named exactly 16 times.
All inputs are finite; a program needn't handle non-finite values.
Results may differ from a plain program's by a relative error of at most 0.013.
Values may be sent and summed in bfloat16 or wider, within the bound.
A program may use at most 64 MiB of HBM per device.

v0:
```python
import functools

import jax
import jax.numpy as jnp
from jax import lax
from jax.experimental import pallas as pl
from jax.experimental.pallas import tpu as pltpu
from jax.sharding import PartitionSpec as P

HEAD_DIM = 64
PIECES = 4
GROUPS = 2


def route_weights(normed, group_router, expert_router, chosen, group_size):
    group_logits = jnp.dot(normed, group_router, preferred_element_type=jnp.float32)
    expert_logits = jnp.dot(normed, expert_router, preferred_element_type=jnp.float32)
    chosen_group = chosen[:, 0] // group_size
    margin = group_logits[:, 0] - group_logits[:, 1]
    own_margin = jnp.where(chosen_group == 0, margin, -margin)
    experts_iota = jnp.arange(expert_logits.shape[1], dtype=jnp.int32)
    picked = jnp.sum(
        jnp.where(
            chosen[:, :, None] == experts_iota[None, None, :],
            expert_logits[:, None, :],
            jnp.float32(0.0),
        ),
        axis=2,
    )
    return jax.nn.sigmoid(own_margin)[:, None] * jax.nn.sigmoid(picked - picked[:, ::-1])


def slot_table(chosen, expert_count, slots):
    flat_ids = chosen.reshape(-1)
    onehot = (flat_ids[:, None] == jnp.arange(expert_count, dtype=jnp.int32)[None, :]).astype(
        jnp.int32
    )
    before = jnp.cumsum(onehot, axis=0) - onehot
    ranks = jnp.sum(before * onehot, axis=1)
    return (flat_ids * slots + ranks).reshape(chosen.shape)


def dispatch(normed, slot_ids, total_slots):
    flat_slots = slot_ids.reshape(-1)
    owners = jnp.arange(flat_slots.shape[0], dtype=jnp.int32) // 2
    slot_iota = jnp.arange(total_slots, dtype=jnp.int32)
    token_of_slot = jnp.sum(
        jnp.where(slot_iota[:, None] == flat_slots[None, :], owners[None, :], 0), axis=1
    )
    return jnp.take(normed, token_of_slot, axis=0)


def expert_rows(row_block, gate_part, up_part, down_part):
    gate_val = jnp.dot(row_block, gate_part, preferred_element_type=jnp.float32)
    up_val = jnp.dot(row_block, up_part, preferred_element_type=jnp.float32)
    hidden = (jax.nn.silu(gate_val) * up_val).astype(jnp.bfloat16)
    return jnp.dot(hidden, down_part, preferred_element_type=jnp.float32).astype(jnp.bfloat16)


MESH_ID = pl.DeviceIdType.MESH
VMEM_SPEC = pl.BlockSpec(memory_space=pltpu.VMEM)
ANY_SPEC = pl.BlockSpec(memory_space=pl.ANY)
F32 = jnp.float32
BF16 = jnp.bfloat16


def remote(src, dst, send_sem, recv_sem, device):
    return pltpu.make_async_remote_copy(
        src_ref=src, dst_ref=dst, send_sem=send_sem, recv_sem=recv_sem,
        device_id=device, device_id_type=MESH_ID,
    )


def columns(piece, width):
    return pl.ds((piece % 2) * (width // 2), width // 2)


def greet(device):
    pl.semaphore_signal(
        pltpu.get_barrier_semaphore(), inc=1, device_id=device, device_id_type=MESH_ID
    )


def line_reduce(chips, chip, sp, tp, block, down_in, up_in, sems, ready=None):
    down_send, down_recv, up_send, up_recv = sems

    def step(dest, half, arrives, inbox, send, recv, device, wait_only):
        piece = block(dest, half)
        copy = remote(piece, inbox.at[dest, half], send.at[dest, half], recv.at[dest, half], device)
        if wait_only:
            copy.wait_send()
            return
        if ready is not None:
            ready(dest, half)

        @pl.when(arrives)
        def _():
            copy.wait_recv()
            piece[...] = (piece[...].astype(F32) + inbox[dest, half].astype(F32)).astype(BF16)

        copy.start()

    def sweep(wait_only):
        for distance in range(chips - 1, 0, -1):
            for half in range(PIECES):

                @pl.when(chip - distance >= 0)
                def _():
                    step(chip - distance, half, chip < chips - 1, down_in, down_send, down_recv,
                         (sp, tp - 2), wait_only)

                @pl.when(chip + distance < chips)
                def _():
                    step(chip + distance, half, chip > 0, up_in, up_send, up_recv,
                         (sp, tp + 2), wait_only)

    sweep(False)
    for half in range(PIECES):
        if ready is not None:
            ready(chip, half)
        piece = block(chip, half)
        for arrives, inbox, recv, send in (
            (chip < chips - 1, down_in, down_recv, down_send),
            (chip > 0, up_in, up_recv, up_send),
        ):

            @pl.when(arrives)
            def _():
                remote(piece, inbox.at[chip, half], send.at[chip, half], recv.at[chip, half],
                       (sp, tp)).wait_recv()
                piece[...] = (piece[...].astype(F32) + inbox[chip, half].astype(F32)).astype(BF16)

    return lambda: sweep(True)


def mixer_kernel(
    sp_count, chips, heads, loads,
    q_ref, k_ref, v_ref, meta_ref, doc_ref, res_ref, gain_ref, w_hbm,
    mixed_ref, normed_ref,
    k_buf, v_buf, m_buf, acc, carry, w_buf, part, partner_in, down_in, up_in,
    w_sem, kv_send, kv_recv, p_send, p_recv, down_send, down_recv, up_send, up_recv,
):
    sp = lax.axis_index("sp")
    tp = lax.axis_index("tp")
    chip = tp // 2
    core = tp % 2
    partner = tp + 1 - 2 * core
    tok, att = q_ref.shape
    width = res_ref.shape[1]
    half_rows = res_ref.shape[0] // 2

    w_copy = pltpu.make_async_copy(w_hbm, w_buf, w_sem)
    w_copy.start()
    for j in range(1, sp_count):
        greet((lax.rem(sp + j, sp_count), tp))
    greet((sp, partner))

    @pl.when(chip > 0)
    def _():
        greet((sp, tp - 2))

    @pl.when(chip < chips - 1)
    def _():
        greet((sp, tp + 2))

    expect = sp_count + jnp.where(chip > 0, 1, 0) + jnp.where(chip < chips - 1, 1, 0)
    for copy in loads:
        copy.wait()
    pl.semaphore_wait(pltpu.get_barrier_semaphore(), expect)

    def kv_copies(j, target):
        return [
            remote(src, buf.at[j - 1], kv_send.at[j - 1, n], kv_recv.at[j - 1, n], (target, tp))
            for n, (src, buf) in enumerate(((k_ref, k_buf), (v_ref, v_buf), (meta_ref, m_buf)))
        ]

    for j in range(1, sp_count):

        @pl.when(sp + j < sp_count)
        def _():
            for copy in kv_copies(j, sp + j):
                copy.start()

    row = lax.broadcasted_iota(jnp.int32, (tok, tok), 0)
    col = lax.broadcasted_iota(jnp.int32, (tok, tok), 1)
    later = jnp.where(row > col, 1.0, 0.0).astype(BF16)
    lane = lax.broadcasted_iota(jnp.int32, (tok, att), 1) // HEAD_DIM
    acc[...] = jnp.zeros_like(acc)
    carry[...] = jnp.zeros_like(carry)

    def attend_block(keys, vals, meta, own):
        live = doc_ref[...] == meta[heads : heads + 1, :]
        if own:
            live = live & (col < row)
        for h in range(heads):
            queries = jnp.where(lane == h, q_ref[...], jnp.zeros((), BF16)) * jnp.asarray(
                HEAD_DIM ** (-0.5), BF16
            )
            scores = lax.dot_general(
                queries, keys, (((1,), (1,)), ((), ())), preferred_element_type=F32
            ) + meta[h : h + 1, :]
            soft = jnp.maximum(scores, 0.0) + jnp.log(1.0 + jnp.exp(-jnp.abs(scores)))
            stay = jnp.where(live, -soft, 0.0)
            high = stay.astype(BF16)
            low = (stay - high.astype(F32)).astype(BF16)
            within = jnp.dot(high, later, preferred_element_type=F32) + jnp.dot(
                low, later, preferred_element_type=F32
            )
            before = carry[h]
            weights = jnp.where(
                live, jnp.exp(scores - soft + within + before), 0.0
            ).astype(BF16)
            out = jnp.dot(weights, vals, preferred_element_type=F32)
            acc[...] += jnp.where(lane == h, out, 0.0)
            carry[h] = before + within[:, :1] + stay[:, :1]

    attend_block(k_ref[...], v_ref[...], meta_ref[...], True)

    def earlier(j, unused):
        @pl.when(sp - j >= 0)
        def _():
            for copy in kv_copies(j, sp):
                copy.wait_recv()
            attend_block(k_buf[j - 1], v_buf[j - 1], m_buf[j - 1], False)

        return unused

    lax.fori_loop(1, sp_count, earlier, 0)
    for j in range(1, sp_count):

        @pl.when(sp + j < sp_count)
        def _():
            for copy in kv_copies(j, sp + j):
                copy.wait_send()

    w_copy.wait()
    attended = acc[...].astype(BF16)
    tile = 512
    for n in range(width // tile):
        cols = slice(n * tile, (n + 1) * tile)
        product = jnp.dot(attended, w_buf[:, cols], preferred_element_type=F32).astype(BF16)
        for z in range(chips):
            for c in range(2):
                for s in range(2):
                    at = ((z * 2 + c) * 2 + s) * half_rows
                    part[c, z, s, :, cols] = product[at : at + half_rows]

    def p_copy(z):
        return remote(
            part.at[1 - core, z], partner_in.at[z], p_send.at[z], p_recv.at[z], (sp, partner)
        )

    for z in range(chips):
        p_copy(z).start()
    for z in range(chips):
        p_copy(z).wait_recv()
        part[core, z] = (part[core, z].astype(F32) + partner_in[z].astype(F32)).astype(BF16)
    finish = line_reduce(
        chips, chip, sp, tp, lambda z, p: part.at[core, z, p // 2, :, columns(p, width)], down_in, up_in,
        (down_send, down_recv, up_send, up_recv),
    )
    total = part[core, chip].reshape(res_ref.shape).astype(F32)
    mixed = (res_ref[...].astype(F32) + total).astype(BF16)
    mixed_ref[...] = mixed
    mixed_f = mixed.astype(F32)
    scaling = lax.rsqrt(jnp.mean(mixed_f * mixed_f, axis=1, keepdims=True) + 1e-06)
    normed_ref[...] = (mixed_f * scaling * gain_ref[...]).astype(BF16)
    for z in range(chips):
        p_copy(z).wait_send()
    finish()


def mixer_inputs(offsets, docs):
    tok, heads = offsets.shape
    docs_f = docs.astype(F32)
    pad = -(heads + 1) % 8
    meta = jnp.concatenate(
        [offsets.astype(F32).T, docs_f[None, :], jnp.zeros((pad, tok), F32)], axis=0
    )
    return meta, docs_f[:, None]


def mixer_scratch(residual, queries, heads, meta, out_weight):
    sp_count = lax.axis_size("sp")
    chips = lax.axis_size("tp") // 2
    rows, width = residual.shape
    tok, att = queries.shape
    others = max(sp_count - 1, 1)
    half = (chips, 2, rows // 2, width)
    quarter = (chips, PIECES, rows // 2, width // 2)
    dma = pltpu.SemaphoreType.DMA
    return [
        pltpu.VMEM((others, tok, att), BF16),
        pltpu.VMEM((others, tok, att), BF16),
        pltpu.VMEM((others,) + meta.shape, F32),
        pltpu.VMEM((tok, att), F32),
        pltpu.VMEM((heads, tok, 1), F32),
        pltpu.VMEM(out_weight.shape, BF16),
        pltpu.VMEM((2,) + half, BF16),
        pltpu.VMEM(half, BF16),
        pltpu.VMEM(quarter, BF16),
        pltpu.VMEM(quarter, BF16),
        dma,
        dma((others, 3)),
        dma((others, 3)),
        dma((chips,)),
        dma((chips,)),
    ] + [dma((chips, PIECES))] * 4


def mixer(residual, queries, keys, values, offsets, docs, out_weight, gain):
    heads = offsets.shape[1]
    meta, doc_column = mixer_inputs(offsets, docs)
    return pl.pallas_call(
        functools.partial(
            mixer_kernel, lax.axis_size("sp"), lax.axis_size("tp") // 2, heads, ()
        ),
        out_shape=[jax.ShapeDtypeStruct(residual.shape, BF16)] * 2,
        in_specs=[VMEM_SPEC] * 7 + [ANY_SPEC],
        out_specs=[VMEM_SPEC] * 2,
        scratch_shapes=mixer_scratch(residual, queries, heads, meta, out_weight),
        compiler_params=pltpu.CompilerParams(
            collective_id=0, has_side_effects=True, vmem_limit_bytes=48 << 20
        ),
        name="mixer",
    )(queries, keys, values, meta, doc_column, residual, gain[None, :], out_weight)


def experts_kernel(
    chips,
    w_copies,
    normed_ref, mixed_ref, sel_ref, sel_t_ref, router_ref,
    out_ref,
    gate, up, down, rows, y_out, part, partner_in, x_in, down_in, up_in, y_in,
    y_sem, rows_recv, line_send, x_send, fan_send,
    p_send, p_recv, xr_send, xr_recv, down_send, down_recv, up_send, up_recv,
):
    sp = lax.axis_index("sp")
    tp = lax.axis_index("tp")
    y, x = sp // 2, sp % 2
    chip, core = tp // 2, tp % 2
    partner = (sp, tp + 1 - 2 * core)
    x_peer = (sp + 1 - 2 * x, tp)
    y_peer = (lax.rem(sp + 2, 4), tp)
    below, above = (sp, tp - 2), (sp, tp + 2)
    has_below, has_above = chip > 0, chip < chips - 1
    half_rows, width = rows.shape[4:]

    own = jnp.dot(sel_ref[y], normed_ref[...], preferred_element_type=F32).astype(BF16)
    other = jnp.dot(sel_ref[1 - y], normed_ref[...], preferred_element_type=F32).astype(BF16)
    rows[x, chip, core, y] = own
    y_out[...] = other

    y_copy = remote(
        y_out, rows.at[x, chip, core, y], y_sem.at[0], rows_recv.at[x, chip, core, y], y_peer
    )
    y_copy.start()

    def piece_copy(xs, z, c, s, send, device):
        piece = rows.at[xs, z, c, s]
        return remote(piece, piece, send, rows_recv.at[xs, z, c, s], device)

    def line_piece(z, s, up_ok, down_ok, act):
        @pl.when(down_ok)
        def _():
            act(piece_copy(x, z, core, s, line_send.at[z, s, 0], below))

        @pl.when(up_ok)
        def _():
            act(piece_copy(x, z, core, s, line_send.at[z, s, 1], above))

        act(piece_copy(x, z, core, s, x_send.at[z, s], x_peer))
        act(piece_copy(x, z, core, s, fan_send.at[0, z, s], partner))

    def begin(copy):
        copy.start()

    def arrived(xs, z, c, s):
        piece_copy(xs, z, c, s, y_sem.at[0], x_peer).wait_recv()

    def own_pieces(act, wait):
        line_piece(chip, y, has_above, has_below, act)
        if wait:
            arrived(x, chip, core, 1 - y)
        line_piece(chip, 1 - y, has_above, has_below, act)

    def line_pieces(distance, act, wait):
        for turn in range(2):
            s = y if turn == 0 else 1 - y

            @pl.when(chip - distance >= 0)
            def _():
                if wait:
                    arrived(x, chip - distance, core, s)
                line_piece(chip - distance, s, has_above, chip < 0, act)

            @pl.when(chip + distance < chips)
            def _():
                if wait:
                    arrived(x, chip + distance, core, s)
                line_piece(chip + distance, s, chip < 0, has_below, act)

    def at_distance(distance, body):
        if distance == 0:
            body(chip)
            return

        @pl.when(chip - distance >= 0)
        def _():
            body(chip - distance)

        @pl.when(chip + distance < chips)
        def _():
            body(chip + distance)

    def cross(z, act, wait):
        for turn in range(2):
            s = y if turn == 0 else 1 - y
            if wait:
                arrived(1 - x, z, core, s)
            act(piece_copy(1 - x, z, core, s, fan_send.at[1, z, s], partner))

    def p_copy(z):
        return remote(part.at[z, 1 - core], partner_in.at[z], p_send.at[z], p_recv.at[z], partner)

    def xr_copy(z, s):
        return remote(
            part.at[z, core, 1 - x, s], x_in.at[z, s], xr_send.at[z, s], xr_recv.at[z, s], x_peer
        )

    lanes = lax.broadcasted_iota(jnp.int32, (1, router_ref.shape[0]), 1)

    def signed(plus, minus):
        return jnp.where(lanes == plus, 1.0, 0.0) - jnp.where(lanes == minus, 1.0, 0.0)

    group_sign = signed(y, 1 - y)
    expert_sign = signed(2 + sp, 2 + sp + 1 - 2 * x)

    def expert(z):
        for xs in range(2):
            for s in range(2):
                arrived(xs, z, 1 - core, s)
        block = rows[:, z].reshape(8 * half_rows, width)
        logits = lax.dot_general(
            block, router_ref[...], (((1,), (1,)), ((), ())), preferred_element_type=F32
        )
        route = jax.nn.sigmoid(
            jnp.sum(logits * group_sign, axis=1, keepdims=True)
        ) * jax.nn.sigmoid(jnp.sum(logits * expert_sign, axis=1, keepdims=True))
        gated = jnp.dot(block, gate[...], preferred_element_type=F32)
        raised = jnp.dot(block, up[...], preferred_element_type=F32)
        hidden = (jax.nn.silu(gated) * raised).astype(BF16)
        tile = 1024
        for n in range(width // tile):
            cols = slice(n * tile, (n + 1) * tile)
            out = jnp.dot(hidden, down[:, cols], preferred_element_type=F32) * route
            out = out.astype(BF16)
            for xs in range(2):
                for c in range(2):
                    for s in range(2):
                        at = ((xs * 2 + c) * 2 + s) * half_rows
                        part[z, c, xs, s, :, cols] = out[at : at + half_rows]
        p_copy(z).start()

    def join_cores(z):
        p_copy(z).wait_recv()
        for xs in (1 - x, x):
            for s in range(2):
                part[z, core, xs, s] = (
                    part[z, core, xs, s].astype(F32) + partner_in[z, xs, s].astype(F32)
                ).astype(BF16)
                if xs is not x:
                    xr_copy(z, s).start()

    def join_x(z, piece):
        s = piece // 2
        if piece % 2 == 0:
            xr_copy(z, s).wait_recv()
            part[z, core, x, s] = (
                part[z, core, x, s].astype(F32) + x_in[z, s].astype(F32)
            ).astype(BF16)

    own_pieces(begin, True)
    for distance in range(1, chips + 1):
        if distance < chips:
            line_pieces(distance, begin, True)
        at_distance(distance - 1, lambda z: cross(z, begin, True))
        if distance == 1:
            for copy in w_copies:
                copy.wait()
        at_distance(distance - 1, expert)
        if distance > 1:
            at_distance(distance - 2, join_cores)
    at_distance(chips - 1, join_cores)
    finish = line_reduce(
        chips, chip, sp, tp, lambda z, p: part.at[z, core, x, p // 2, :, columns(p, width)], down_in, up_in,
        (down_send, down_recv, up_send, up_recv), join_x,
    )
    y_back = remote(part.at[chip, core, x, 1 - y], y_in, y_sem.at[1], y_sem.at[2], y_peer)
    y_back.start()
    result = mixed_ref[...].astype(F32) + jnp.dot(
        sel_t_ref[y], part[chip, core, x, y], preferred_element_type=F32
    )
    y_back.wait_recv()
    result = result + jnp.dot(sel_t_ref[1 - y], y_in[...], preferred_element_type=F32)
    out_ref[...] = result.astype(BF16)

    def end(copy):
        copy.wait_send()

    y_back.wait_send()
    y_copy.wait_send()
    own_pieces(end, False)
    for distance in range(chips):
        if distance:
            line_pieces(distance, end, False)
        at_distance(distance, lambda z: cross(z, end, False))
        at_distance(distance, lambda z: end(p_copy(z)))
        for s in range(2):
            at_distance(distance, lambda z: end(xr_copy(z, s)))
    finish()


def layer_kernel(
    sp_count, chips, heads, mixer_count,
    q_hbm, k_hbm, v_hbm, res_hbm, w_hbm, gate_hbm, up_hbm, down_hbm,
    meta_ref, doc_ref, gain_ref, sel_ref, sel_t_ref, router_ref,
    out_ref,
    q_ref, k_ref, v_ref, res_ref, mixed_ref, normed_ref, load_sem, weight_sem, gate, up, down,
    *scratch,
):
    loads = [
        pltpu.make_async_copy(src, dst, load_sem.at[n])
        for n, (src, dst) in enumerate(
            ((k_hbm, k_ref), (v_hbm, v_ref), (q_hbm, q_ref), (res_hbm, res_ref))
        )
    ]
    weights = [
        pltpu.make_async_copy(src.at[0], dst, weight_sem.at[n])
        for n, (src, dst) in enumerate(((gate_hbm, gate), (up_hbm, up), (down_hbm, down)))
    ]
    for copy in loads + weights:
        copy.start()
    mixer_kernel(
        sp_count, chips, heads, loads,
        q_ref, k_ref, v_ref, meta_ref, doc_ref, res_ref, gain_ref, w_hbm,
        mixed_ref, normed_ref, *scratch[:mixer_count],
    )
    experts_kernel(
        chips, weights, normed_ref, mixed_ref, sel_ref, sel_t_ref, router_ref, out_ref,
        gate, up, down, *scratch[mixer_count:],
    )


def pair_layer(
    residual, queries, keys, values, offsets, docs, out_weight, gain,
    chosen, group_router, expert_router, gate, up, down,
):
    chips = lax.axis_size("tp") // 2
    rows, width = residual.shape
    heads = offsets.shape[1]
    meta, doc_column = mixer_inputs(offsets, docs)
    mixer_parts = mixer_scratch(residual, queries, heads, meta, out_weight)
    half_rows = rows // 2
    group = chosen[:, 0] // 2
    token = jnp.arange(rows, dtype=jnp.int32)
    rank = jnp.sum(
        ((group[None, :] == group[:, None]) & (token[None, :] < token[:, None])).astype(jnp.int32),
        axis=1,
    )
    slot = group * half_rows + rank
    sel = (token[:, None] == slot[None, :]).astype(BF16)
    sel_t = (
        slot[None, :, None] == token.reshape(2, 1, half_rows)
    ).astype(BF16)
    router = jnp.concatenate(
        [group_router.T, expert_router.T, jnp.zeros((2, width), BF16)], axis=0
    )
    units = gate.shape[2]
    half = (chips, 2, half_rows, width)
    quarter = (chips, PIECES, half_rows, width // 2)
    dma = pltpu.SemaphoreType.DMA
    return pl.pallas_call(
        functools.partial(
            layer_kernel, lax.axis_size("sp"), chips, heads, len(mixer_parts)
        ),
        out_shape=jax.ShapeDtypeStruct((rows, width), BF16),
        in_specs=[ANY_SPEC] * 8 + [VMEM_SPEC] * 6,
        out_specs=VMEM_SPEC,
        scratch_shapes=[
            pltpu.VMEM(queries.shape, BF16),
            pltpu.VMEM(keys.shape, BF16),
            pltpu.VMEM(values.shape, BF16),
            pltpu.VMEM((rows, width), BF16),
            pltpu.VMEM((rows, width), BF16),
            pltpu.VMEM((rows, width), BF16),
            dma((4,)),
            dma((3,)),
            pltpu.VMEM((width, units), BF16),
            pltpu.VMEM((width, units), BF16),
            pltpu.VMEM((units, width), BF16),
        ]
        + mixer_parts
        + [
            pltpu.VMEM((2, chips, 2, 2, half_rows, width), BF16),
            pltpu.VMEM((half_rows, width), BF16),
            pltpu.VMEM((chips, 2, 2, 2, half_rows, width), BF16),
            pltpu.VMEM((chips, 2, 2, half_rows, width), BF16),
            pltpu.VMEM(half, BF16),
            pltpu.VMEM(quarter, BF16),
            pltpu.VMEM(quarter, BF16),
            pltpu.VMEM((half_rows, width), BF16),
            dma((3,)),
            dma((2, chips, 2, 2)),
            dma((chips, 2, 2)),
            dma((chips, 2)),
            dma((2, chips, 2)),
            dma((chips,)),
            dma((chips,)),
            dma((chips, 2)),
            dma((chips, 2)),
        ]
        + [dma((chips, PIECES))] * 4,
        compiler_params=pltpu.CompilerParams(
            collective_id=1, has_side_effects=True, vmem_limit_bytes=60 << 20
        ),
        name="layer",
    )(
        queries, keys, values, residual, out_weight, gate, up, down,
        meta, doc_column, gain[None, :], sel.reshape(2, half_rows, rows), sel_t, router,
    )


def per_device(
    residual_in,
    queries,
    keys,
    values,
    break_offset,
    doc_ids,
    out_weight,
    norm_gain,
    group_router,
    expert_router,
    expert_ids,
    gate_weight,
    up_weight,
    down_weight,
):
    tok_dev = queries.shape[0]
    sp_count = lax.axis_size("sp")
    tp_count = lax.axis_size("tp")
    tp_rank = lax.axis_index("tp")
    width = residual_in.shape[1]
    rows_dev = tok_dev // tp_count
    chosen = lax.dynamic_slice_in_dim(expert_ids, tp_rank * rows_dev, rows_dev, 0)
    expert_count = sp_count * gate_weight.shape[0]
    group_size = expert_count // GROUPS
    if sp_count == 4 and gate_weight.shape[0] == 1 and rows_dev % 32 == 0:
        return pair_layer(
            residual_in, queries, keys, values, break_offset, doc_ids, out_weight, norm_gain,
            chosen, group_router, expert_router, gate_weight, up_weight, down_weight,
        )
    mixed_stream, normed = mixer(
        residual_in, queries, keys, values, break_offset, doc_ids, out_weight, norm_gain
    )
    routes = route_weights(normed, group_router, expert_router, chosen, group_size)
    slots = 2 * rows_dev // expert_count
    slot_ids = slot_table(chosen, expert_count, slots)
    sent = dispatch(normed, slot_ids, expert_count * slots).reshape(expert_count, slots, width)
    fanned = lax.all_gather(
        lax.all_to_all(sent, "sp", split_axis=0, concat_axis=0, tiled=True),
        "tp",
        axis=0,
        tiled=True,
    )
    partial_out = expert_rows(
        fanned.reshape(-1, width), gate_weight[0], up_weight[0], down_weight[0]
    )
    unit_total = lax.psum_scatter(
        partial_out.reshape(fanned.shape), "tp", scatter_dimension=0, tiled=True
    ).astype(jnp.float32)
    returned = lax.all_to_all(
        unit_total.astype(jnp.bfloat16), "sp", split_axis=0, concat_axis=0, tiled=True
    )
    expert_out = jnp.take(returned.reshape(-1, width), slot_ids.reshape(-1), axis=0).reshape(
        rows_dev, 2, width
    )
    mixture = jnp.sum(routes[:, :, None] * expert_out.astype(jnp.float32), axis=1)
    return (mixed_stream.astype(jnp.float32) + mixture).astype(jnp.bfloat16)


def solution(mesh):
    return jax.shard_map(
        per_device,
        mesh=mesh,
        in_specs=(
            P(("sp", "tp"), None),
            P("sp", "tp"),
            P("sp", "tp"),
            P("sp", "tp"),
            P("sp", "tp"),
            P("sp"),
            P("tp", None),
            P(),
            P(),
            P(),
            P("sp", None),
            P("sp", None, "tp"),
            P("sp", None, "tp"),
            P("sp", "tp", None),
        ),
        out_specs=P(("sp", "tp"), None),
        check_vma=False,
    )
```

profile of v0, /device:TPU:20, one launch (start us, length us, event | category | flops | bytes accessed | tf_op | source)
XLA Modules:
  0.0 124.6 jit_solution(17220222276471806892)
XLA Ops:
  0.0 0.0 copy-start
  0.0 0.7 copy-done
  0.7 0.1 constant_dynamic-slice_fusion
  0.8 0.2 convert_reduce_fusion
  1.0 0.1 pad.5.clone
  1.1 0.1 pad.2.clone
  1.1 0.7 convert_element_type.14
  1.8 0.7 convert_bitcast_fusion
  2.5 0.7 maximum_maximum_fusion.1.meta_ref
  3.2 0.7 compare_convert_fusion.1.sel_ref
  3.8 0.7 compare_convert_fusion.sel_t_ref
  4.5 1.5 %maximum_maximum_fusion.router_ref = bf16[8,4096]{1,0:T(8,128)(2,1)} fusion(bf16[4,4096]{1,0:T(4,128)(2,1)} %bitcast.19, bf16[2,4096]{1,0:T(2,128)(2,1)} %bitcast.21, bf16[8]{0:T(256)(128)(2,1)S(1)} %pad.2.clone), kind=kLoop, calls=%fused_computation | loop fusion | flops 196608 | bytes 114704 | tf_op jit(solution)/shard_map/concatenate | solution.py:576
  6.0 0.8 copy.16.doc_ref
  6.8 116.1 %layer.1 = bf16[32,4096]{1,0:T(8,128)(2,1)} custom-call(bf16[256,256]{1,0:T(8,128)(2,1)} %q_hbm.1, bf16[256,256]{1,0:T(8,128)(2,1)} %k_hbm.1, bf16[256,256]{1,0:T(8,128)(2,1)} %v_hbm.1, bf16[32,4096]{1,0:T(8,128)(2,1)} %res_hbm.1, bf16[256,4096]{1,0:T(8,128)(2,1)} %w_hbm.1, bf16[1,4096,512]{2,1,0:T(8,128)(2,1)} %gate_hbm.1, bf16[1,4096,512]{2,1,0:T(8,128)(2,1)} %up_hbm.1, ...), custom_call_target="tpu_custom_call" | custom-call | tf_op jit(solution)/shard_map/layer/pallas_call | solution.py:583
  122.9 1.7 %copy.18 = bf16[32,4096]{1,0:T(8,128)(2,1)} copy(bf16[32,4096]{1,0:T(8,128)(2,1)} %layer.1) | data formatting | bytes 524288
  (6 shorter events, 0.0 us)
Async XLA Ops:
  0.0 0.7 copy-start
where the time goes:
time: 125 us
  Pallas kernels  116 us (93%)
  other arithmetic  5.04 us (4%)
  local copies, waits for them, and re-layouts  3.38 us (3%)
    pallas_call x1, Pallas kernels, pair_layer(): pl.pallas_call(functools.partial(layer_kernel, lax.axis_size('sp'), chips...  116 us

commit v1 on v0

--- a/solution.py
+++ b/solution.py
@@ -81,7 +81,9 @@
     )
 
 
-def line_reduce(chips, chip, sp, tp, block, down_in, up_in, sems, ready=None):
+def line_reduce(
+    chips, chip, sp, tp, block, down_in, up_in, sems, ready=None, finished=None, near_first=False
+):
     down_send, down_recv, up_send, up_recv = sems
 
     def step(dest, half, arrives, inbox, send, recv, device, wait_only):
@@ -101,17 +103,21 @@
         copy.start()
 
     def sweep(wait_only):
-        for distance in range(chips - 1, 0, -1):
+        for turn in range(1, 2 * chips - 2 if near_first else chips):
+            if near_first:
+                below, above = 2 * (chips - 1) - turn - chip, turn - chip
+            else:
+                below, above = chip - (chips - turn), chip + (chips - turn)
             for half in range(PIECES):
 
-                @pl.when(chip - distance >= 0)
+                @pl.when((below >= 0) & (below < chip))
                 def _():
-                    step(chip - distance, half, chip < chips - 1, down_in, down_send, down_recv,
+                    step(below, half, chip < chips - 1, down_in, down_send, down_recv,
                          (sp, tp - 2), wait_only)
 
-                @pl.when(chip + distance < chips)
+                @pl.when((above > chip) & (above < chips))
                 def _():
-                    step(chip + distance, half, chip > 0, up_in, up_send, up_recv,
+                    step(above, half, chip > 0, up_in, up_send, up_recv,
                          (sp, tp + 2), wait_only)
 
     sweep(False)
@@ -130,14 +136,17 @@
                        (sp, tp)).wait_recv()
                 piece[...] = (piece[...].astype(F32) + inbox[chip, half].astype(F32)).astype(BF16)
 
+        if finished is not None:
+            finished(half)
+
     return lambda: sweep(True)
 
 
 def mixer_kernel(
-    sp_count, chips, heads, loads,
-    q_ref, k_ref, v_ref, meta_ref, doc_ref, res_ref, gain_ref, w_hbm,
+    sp_count, chips, heads, loads, later_loads,
+    q_ref, k_ref, v_ref, off_ref, doc_ref, res_ref, gain_ref, w_hbm,
     mixed_ref, normed_ref,
-    k_buf, v_buf, m_buf, acc, carry, w_buf, part, partner_in, down_in, up_in,
+    meta_ref, doc_col, k_buf, v_buf, m_buf, acc, carry, w_buf, part, partner_in, down_in, up_in,
     w_sem, kv_send, kv_recv, p_send, p_recv, down_send, down_recv, up_send, up_recv,
 ):
     sp = lax.axis_index("sp")
@@ -150,7 +159,6 @@
     half_rows = res_ref.shape[0] // 2
 
     w_copy = pltpu.make_async_copy(w_hbm, w_buf, w_sem)
-    w_copy.start()
     for j in range(1, sp_count):
         greet((lax.rem(sp + j, sp_count), tp))
     greet((sp, partner))
@@ -164,6 +172,11 @@
         greet((sp, tp + 2))
 
     expect = sp_count + jnp.where(chip > 0, 1, 0) + jnp.where(chip < chips - 1, 1, 0)
+    docs = doc_ref[...].astype(F32)
+    meta_ref[...] = jnp.zeros_like(meta_ref)
+    meta_ref[0:heads, :] = off_ref[...].astype(F32)
+    meta_ref[heads : heads + 1, :] = docs
+    doc_col[...] = jnp.broadcast_to(docs, (128, tok)).T[:, :1]
     for copy in loads:
         copy.wait()
     pl.semaphore_wait(pltpu.get_barrier_semaphore(), expect)
@@ -180,6 +193,10 @@
         def _():
             for copy in kv_copies(j, sp + j):
                 copy.start()
+
+    w_copy.start()
+    for copy in later_loads:
+        copy.start()
 
     row = lax.broadcasted_iota(jnp.int32, (tok, tok), 0)
     col = lax.broadcasted_iota(jnp.int32, (tok, tok), 1)
@@ -189,7 +206,7 @@
     carry[...] = jnp.zeros_like(carry)
 
     def attend_block(keys, vals, meta, own):
-        live = doc_ref[...] == meta[heads : heads + 1, :]
+        live = doc_col[...] == meta[heads : heads + 1, :]
         if own:
             live = live & (col < row)
         for h in range(heads):
@@ -259,6 +276,8 @@
         chips, chip, sp, tp, lambda z, p: part.at[core, z, p // 2, :, columns(p, width)], down_in, up_in,
         (down_send, down_recv, up_send, up_recv),
     )
+    for copy in later_loads[:1]:
+        copy.wait()
     total = part[core, chip].reshape(res_ref.shape).astype(F32)
     mixed = (res_ref[...].astype(F32) + total).astype(BF16)
     mixed_ref[...] = mixed
@@ -270,17 +289,7 @@
     finish()
 
 
-def mixer_inputs(offsets, docs):
-    tok, heads = offsets.shape
-    docs_f = docs.astype(F32)
-    pad = -(heads + 1) % 8
-    meta = jnp.concatenate(
-        [offsets.astype(F32).T, docs_f[None, :], jnp.zeros((pad, tok), F32)], axis=0
-    )
-    return meta, docs_f[:, None]
-
-
-def mixer_scratch(residual, queries, heads, meta, out_weight):
+def mixer_scratch(residual, queries, heads, out_weight):
     sp_count = lax.axis_size("sp")
     chips = lax.axis_size("tp") // 2
     rows, width = residual.shape
@@ -289,10 +298,13 @@
     half = (chips, 2, rows // 2, width)
     quarter = (chips, PIECES, rows // 2, width // 2)
     dma = pltpu.SemaphoreType.DMA
+    meta_shape = (heads + 1 + -(heads + 1) % 8, tok)
     return [
+        pltpu.VMEM(meta_shape, F32),
+        pltpu.VMEM((tok, 1), F32),
         pltpu.VMEM((others, tok, att), BF16),
         pltpu.VMEM((others, tok, att), BF16),
-        pltpu.VMEM((others,) + meta.shape, F32),
+        pltpu.VMEM((others,) + meta_shape, F32),
         pltpu.VMEM((tok, att), F32),
         pltpu.VMEM((heads, tok, 1), F32),
         pltpu.VMEM(out_weight.shape, BF16),
@@ -310,28 +322,43 @@
 
 def mixer(residual, queries, keys, values, offsets, docs, out_weight, gain):
     heads = offsets.shape[1]
-    meta, doc_column = mixer_inputs(offsets, docs)
     return pl.pallas_call(
         functools.partial(
-            mixer_kernel, lax.axis_size("sp"), lax.axis_size("tp") // 2, heads, ()
+            mixer_kernel, lax.axis_size("sp"), lax.axis_size("tp") // 2, heads, (), ()
         ),
         out_shape=[jax.ShapeDtypeStruct(residual.shape, BF16)] * 2,
         in_specs=[VMEM_SPEC] * 7 + [ANY_SPEC],
         out_specs=[VMEM_SPEC] * 2,
-        scratch_shapes=mixer_scratch(residual, queries, heads, meta, out_weight),
+        scratch_shapes=mixer_scratch(residual, queries, heads, out_weight),
         compiler_params=pltpu.CompilerParams(
             collective_id=0, has_side_effects=True, vmem_limit_bytes=48 << 20
         ),
         name="mixer",
-    )(queries, keys, values, meta, doc_column, residual, gain[None, :], out_weight)
+    )(queries, keys, values, offsets.T, docs[None, :], residual, gain[None, :], out_weight)
+
+
+def slot_row(ids, tp, rows):
+    tok = ids.shape[1]
+    group = jnp.broadcast_to((ids[:1, :] // 2).astype(F32), (8, tok)).astype(BF16)
+    at = lax.broadcasted_iota(jnp.int32, (tok, 128), 0)
+    lane = lax.broadcasted_iota(jnp.int32, (tok, 128), 1)
+    pick = jnp.where(at == lane + tp * rows, 1.0, 0.0).astype(BF16)
+    mine = jnp.dot(group, pick, preferred_element_type=F32)
+    before_at = lax.broadcasted_iota(jnp.int32, (128, 128), 0)
+    before_lane = lax.broadcasted_iota(jnp.int32, (128, 128), 1)
+    before = jnp.where(before_at < before_lane, 1.0, 0.0).astype(BF16)
+    ones = jnp.dot(mine.astype(BF16), before, preferred_element_type=F32)
+    token = lax.broadcasted_iota(jnp.int32, (8, 128), 1).astype(F32)
+    slot = jnp.where(mine > 0.5, ones + rows // 2, token - ones)
+    return slot[:1, :rows]
 
 
 def experts_kernel(
     chips,
     w_copies,
-    normed_ref, mixed_ref, sel_ref, sel_t_ref, router_ref,
+    normed_ref, mixed_ref, ids_ref, group_ref, expert_ref,
     out_ref,
-    gate, up, down, rows, y_out, part, partner_in, x_in, down_in, up_in, y_in,
+    router_ref, gate, up, down, rows, y_out, part, partner_in, x_in, down_in, up_in, y_in, total,
     y_sem, rows_recv, line_send, x_send, fan_send,
     p_send, p_recv, xr_send, xr_recv, down_send, down_recv, up_send, up_recv,
 ):
@@ -346,8 +373,20 @@
     has_below, has_above = chip > 0, chip < chips - 1
     half_rows, width = rows.shape[4:]
 
-    own = jnp.dot(sel_ref[y], normed_ref[...], preferred_element_type=F32).astype(BF16)
-    other = jnp.dot(sel_ref[1 - y], normed_ref[...], preferred_element_type=F32).astype(BF16)
+    row_count = 2 * half_rows
+    slots = slot_row(ids_ref[...], tp, row_count)
+    slot_iota = lax.broadcasted_iota(jnp.int32, (half_rows, row_count), 0)
+
+    def selection(group):
+        wanted = (slot_iota + group * half_rows).astype(F32)
+        return jnp.where(wanted == slots, 1.0, 0.0).astype(BF16)
+
+    sel_own, sel_other = selection(y), selection(1 - y)
+    router_ref[...] = jnp.zeros_like(router_ref)
+    router_ref[0:2, :] = group_ref[...].astype(F32)
+    router_ref[2:6, :] = expert_ref[...].astype(F32)
+    own = jnp.dot(sel_own, normed_ref[...], preferred_element_type=F32).astype(BF16)
+    other = jnp.dot(sel_other, normed_ref[...], preferred_element_type=F32).astype(BF16)
     rows[x, chip, core, y] = own
     y_out[...] = other
 
@@ -442,7 +481,7 @@
                 arrived(xs, z, 1 - core, s)
         block = rows[:, z].reshape(8 * half_rows, width)
         logits = lax.dot_general(
-            block, router_ref[...], (((1,), (1,)), ((), ())), preferred_element_type=F32
+            block, router_ref[...].astype(BF16), (((1,), (1,)), ((), ())), preferred_element_type=F32
         )
         route = jax.nn.sigmoid(
             jnp.sum(logits * group_sign, axis=1, keepdims=True)
@@ -462,23 +501,43 @@
                         part[z, c, xs, s, :, cols] = out[at : at + half_rows]
         p_copy(z).start()
 
-    def join_cores(z):
+    halves = (1 - y, y)
+
+    def join_cores(z, send=True):
         p_copy(z).wait_recv()
         for xs in (1 - x, x):
-            for s in range(2):
+            for s in halves:
                 part[z, core, xs, s] = (
                     part[z, core, xs, s].astype(F32) + partner_in[z, xs, s].astype(F32)
                 ).astype(BF16)
-                if xs is not x:
+                if xs is not x and send:
                     xr_copy(z, s).start()
 
     def join_x(z, piece):
-        s = piece // 2
+        s = halves[piece // 2]
         if piece % 2 == 0:
             xr_copy(z, s).wait_recv()
             part[z, core, x, s] = (
                 part[z, core, x, s].astype(F32) + x_in[z, s].astype(F32)
             ).astype(BF16)
+
+    def back_copy(n):
+        cols = columns(n, width)
+        return remote(
+            part.at[chip, core, x, 1 - y, :, cols], y_in.at[:, cols], y_sem.at[1 + n],
+            y_sem.at[3 + n], y_peer,
+        )
+
+    def finished(piece):
+        cols = columns(piece, width)
+        if piece < 2:
+            back_copy(piece).start()
+        else:
+            sums = lax.dot_general(
+                sel_own, part[chip, core, x, y, :, cols], (((0,), (0,)), ((), ())),
+                preferred_element_type=F32,
+            )
+            total[:, cols] = mixed_ref[:, cols].astype(F32) + sums
 
     own_pieces(begin, True)
     for distance in range(1, chips + 1):
@@ -490,25 +549,28 @@
                 copy.wait()
         at_distance(distance - 1, expert)
         if distance > 1:
-            at_distance(distance - 2, join_cores)
+            at_distance(distance - 2, lambda z: join_cores(z, distance > 2))
     at_distance(chips - 1, join_cores)
+    for s in halves:
+        xr_copy(chip, s).start()
     finish = line_reduce(
-        chips, chip, sp, tp, lambda z, p: part.at[z, core, x, p // 2, :, columns(p, width)], down_in, up_in,
-        (down_send, down_recv, up_send, up_recv), join_x,
-    )
-    y_back = remote(part.at[chip, core, x, 1 - y], y_in, y_sem.at[1], y_sem.at[2], y_peer)
-    y_back.start()
-    result = mixed_ref[...].astype(F32) + jnp.dot(
-        sel_t_ref[y], part[chip, core, x, y], preferred_element_type=F32
-    )
-    y_back.wait_recv()
-    result = result + jnp.dot(sel_t_ref[1 - y], y_in[...], preferred_element_type=F32)
-    out_ref[...] = result.astype(BF16)
+        chips, chip, sp, tp,
+        lambda z, p: part.at[z, core, x, halves[p // 2], :, columns(p, width)],
+        down_in, up_in, (down_send, down_recv, up_send, up_recv), join_x, finished, True,
+    )
+    for n in range(2):
+        cols = columns(n, width)
+        back_copy(n).wait_recv()
+        sums = lax.dot_general(
+            sel_other, y_in[:, cols], (((0,), (0,)), ((), ())), preferred_element_type=F32
+        )
+        out_ref[:, cols] = (total[:, cols] + sums).astype(BF16)
 
     def end(copy):
         copy.wait_send()
 
-    y_back.wait_send()
+    for n in range(2):
+        back_copy(n).wait_send()
     y_copy.wait_send()
     own_pieces(end, False)
     for distance in range(chips):
@@ -524,9 +586,10 @@
 def layer_kernel(
     sp_count, chips, heads, mixer_count,
     q_hbm, k_hbm, v_hbm, res_hbm, w_hbm, gate_hbm, up_hbm, down_hbm,
-    meta_ref, doc_ref, gain_ref, sel_ref, sel_t_ref, router_ref,
+    off_ref, doc_ref, gain_ref, ids_ref, group_ref, expert_ref,
     out_ref,
-    q_ref, k_ref, v_ref, res_ref, mixed_ref, normed_ref, load_sem, weight_sem, gate, up, down,
+    q_ref, k_ref, v_ref, res_ref, mixed_ref, normed_ref, load_sem, weight_sem, router_ref,
+    gate, up, down,
     *scratch,
 ):
     loads = [
@@ -539,43 +602,28 @@
         pltpu.make_async_copy(src.at[0], dst, weight_sem.at[n])
         for n, (src, dst) in enumerate(((gate_hbm, gate), (up_hbm, up), (down_hbm, down)))
     ]
-    for copy in loads + weights:
+    for copy in loads[:3]:
         copy.start()
     mixer_kernel(
-        sp_count, chips, heads, loads,
-        q_ref, k_ref, v_ref, meta_ref, doc_ref, res_ref, gain_ref, w_hbm,
+        sp_count, chips, heads, loads[:3], loads[3:] + weights,
+        q_ref, k_ref, v_ref, off_ref, doc_ref, res_ref, gain_ref, w_hbm,
         mixed_ref, normed_ref, *scratch[:mixer_count],
     )
     experts_kernel(
-        chips, weights, normed_ref, mixed_ref, sel_ref, sel_t_ref, router_ref, out_ref,
-        gate, up, down, *scratch[mixer_count:],
+        chips, weights, normed_ref, mixed_ref, ids_ref, group_ref, expert_ref, out_ref,
+        router_ref, gate, up, down, *scratch[mixer_count:],
     )
 
 
 def pair_layer(
     residual, queries, keys, values, offsets, docs, out_weight, gain,
-    chosen, group_router, expert_router, gate, up, down,
+    expert_ids, group_router, expert_router, gate, up, down,
 ):
     chips = lax.axis_size("tp") // 2
     rows, width = residual.shape
     heads = offsets.shape[1]
-    meta, doc_column = mixer_inputs(offsets, docs)
-    mixer_parts = mixer_scratch(residual, queries, heads, meta, out_weight)
+    mixer_parts = mixer_scratch(residual, queries, heads, out_weight)
     half_rows = rows // 2
-    group = chosen[:, 0] // 2
-    token = jnp.arange(rows, dtype=jnp.int32)
-    rank = jnp.sum(
-        ((group[None, :] == group[:, None]) & (token[None, :] < token[:, None])).astype(jnp.int32),
-        axis=1,
-    )
-    slot = group * half_rows + rank
-    sel = (token[:, None] == slot[None, :]).astype(BF16)
-    sel_t = (
-        slot[None, :, None] == token.reshape(2, 1, half_rows)
-    ).astype(BF16)
-    router = jnp.concatenate(
-        [group_router.T, expert_router.T, jnp.zeros((2, width), BF16)], axis=0
-    )
     units = gate.shape[2]
     half = (chips, 2, half_rows, width)
     quarter = (chips, PIECES, half_rows, width // 2)
@@ -596,6 +644,7 @@
             pltpu.VMEM((rows, width), BF16),
             dma((4,)),
             dma((3,)),
+            pltpu.VMEM((8, width), F32),
             pltpu.VMEM((width, units), BF16),
             pltpu.VMEM((width, units), BF16),
             pltpu.VMEM((units, width), BF16),
@@ -610,7 +659,8 @@
             pltpu.VMEM(quarter, BF16),
             pltpu.VMEM(quarter, BF16),
             pltpu.VMEM((half_rows, width), BF16),
-            dma((3,)),
+            pltpu.VMEM((rows, width), F32),
+            dma((5,)),
             dma((2, chips, 2, 2)),
             dma((chips, 2, 2)),
             dma((chips, 2)),
@@ -627,7 +677,7 @@
         name="layer",
     )(
         queries, keys, values, residual, out_weight, gate, up, down,
-        meta, doc_column, gain[None, :], sel.reshape(2, half_rows, rows), sel_t, router,
+        offsets.T, docs[None, :], gain[None, :], expert_ids.T, group_router.T, expert_router.T,
     )
 
 
@@ -659,7 +709,7 @@
     if sp_count == 4 and gate_weight.shape[0] == 1 and rows_dev % 32 == 0:
         return pair_layer(
             residual_in, queries, keys, values, break_offset, doc_ids, out_weight, norm_gain,
-            chosen, group_router, expert_router, gate_weight, up_weight, down_weight,
+            expert_ids, group_router, expert_router, gate_weight, up_weight, down_weight,
         )
     mixed_stream, normed = mixer(
         residual_in, queries, keys, values, break_offset, doc_ids, out_weight, norm_gain

time: 125 us -> 109 us (0.87)
  the two profiles are of different devices: /device:TPU:20 before, /device:TPU:0 now
where the time goes in v1:
time: 109 us; the launch traced here: 108 us
  Pallas kernels  107 us (98%)
  local copies, waits for them, and re-layouts  1.67 us (2%)
    pallas_call x1, Pallas kernels, pair_layer(): pl.pallas_call(functools.partial(layer_kernel, lax.axis_size('sp'), chips...  107 us

profile of v1, /device:TPU:0, one launch (start us, length us, event | category | flops | bytes accessed | tf_op | source)
XLA Modules:
  0.0 108.4 jit_solution(7434723209921373911)
XLA Ops:
  0.0 106.8 %layer.1 = bf16[32,4096]{1,0:T(8,128)(2,1)} custom-call(bf16[256,256]{1,0:T(8,128)(2,1)} %q_hbm.1, bf16[256,256]{1,0:T(8,128)(2,1)} %k_hbm.1, bf16[256,256]{1,0:T(8,128)(2,1)} %v_hbm.1, bf16[32,4096]{1,0:T(8,128)(2,1)} %res_hbm.1, bf16[256,4096]{1,0:T(8,128)(2,1)} %w_hbm.1, bf16[1,4096,512]{2,1,0:T(8,128)(2,1)} %gate_hbm.1, bf16[1,4096,512]{2,1,0:T(8,128)(2,1)} %up_hbm.1, ...), custom_call_target="tpu_custom_call" | custom-call | tf_op jit(solution)/shard_map/layer/pallas_call | solution.py:631
  106.8 1.7 %copy.16 = bf16[32,4096]{1,0:T(8,128)(2,1)} copy(bf16[32,4096]{1,0:T(8,128)(2,1)} %layer.1) | data formatting | bytes 524288

commit v2 on v1

--- a/solution.py
+++ b/solution.py
@@ -81,73 +81,61 @@
     )
 
 
-def line_reduce(
-    chips, chip, sp, tp, block, down_in, up_in, sems, ready=None, finished=None, near_first=False
-):
-    down_send, down_recv, up_send, up_recv = sems
-
-    def step(dest, half, arrives, inbox, send, recv, device, wait_only):
-        piece = block(dest, half)
-        copy = remote(piece, inbox.at[dest, half], send.at[dest, half], recv.at[dest, half], device)
-        if wait_only:
-            copy.wait_send()
-            return
-        if ready is not None:
-            ready(dest, half)
-
-        @pl.when(arrives)
+class Line:
+    def __init__(self, chips, chip, sp, tp, block, down_in, up_in, sems):
+        self.chips, self.chip, self.me, self.block = chips, chip, (sp, tp), block
+        down_send, down_recv, up_send, up_recv = sems
+        self.legs = (
+            (down_in, down_send, down_recv, (sp, tp - 2), chip < chips - 1),
+            (up_in, up_send, up_recv, (sp, tp + 2), chip > 0),
+        )
+
+    def copy(self, leg, dest, p, device):
+        inbox, send, recv = leg[:3]
+        return remote(
+            self.block(dest, p), inbox.at[dest, p], send.at[dest, p], recv.at[dest, p], device
+        )
+
+    def gather(self, leg, dest, p, device):
+        @pl.when(leg[4])
         def _():
-            copy.wait_recv()
-            piece[...] = (piece[...].astype(F32) + inbox[dest, half].astype(F32)).astype(BF16)
-
-        copy.start()
-
-    def sweep(wait_only):
-        for turn in range(1, 2 * chips - 2 if near_first else chips):
-            if near_first:
-                below, above = 2 * (chips - 1) - turn - chip, turn - chip
-            else:
-                below, above = chip - (chips - turn), chip + (chips - turn)
-            for half in range(PIECES):
-
-                @pl.when((below >= 0) & (below < chip))
+            self.copy(leg, dest, p, device).wait_recv()
+            piece = self.block(dest, p)
+            piece[...] = (piece[...].astype(F32) + leg[0][dest, p].astype(F32)).astype(BF16)
+
+    def send(self, below, above, pieces, ready):
+        chip, chips = self.chip, self.chips
+        for p in pieces:
+            for leg, dest, valid in (
+                (self.legs[0], below, (below >= 0) & (below < chip)),
+                (self.legs[1], above, (above > chip) & (above < chips)),
+            ):
+
+                @pl.when(valid)
                 def _():
-                    step(below, half, chip < chips - 1, down_in, down_send, down_recv,
-                         (sp, tp - 2), wait_only)
-
-                @pl.when((above > chip) & (above < chips))
+                    ready(dest, p)
+                    self.gather(leg, dest, p, leg[3])
+                    self.copy(leg, dest, p, leg[3]).start()
+
+    def own(self, p, ready):
+        ready(self.chip, p)
+        for leg in self.legs:
+            self.gather(leg, self.chip, p, leg[3])
+
+    def drain(self):
+        for dest in range(self.chips):
+            for leg, sent in ((self.legs[0], dest < self.chip), (self.legs[1], dest > self.chip)):
+
+                @pl.when(sent)
                 def _():
-                    step(above, half, chip > 0, up_in, up_send, up_recv,
-                         (sp, tp + 2), wait_only)
-
-    sweep(False)
-    for half in range(PIECES):
-        if ready is not None:
-            ready(chip, half)
-        piece = block(chip, half)
-        for arrives, inbox, recv, send in (
-            (chip < chips - 1, down_in, down_recv, down_send),
-            (chip > 0, up_in, up_recv, up_send),
-        ):
-
-            @pl.when(arrives)
-            def _():
-                remote(piece, inbox.at[chip, half], send.at[chip, half], recv.at[chip, half],
-                       (sp, tp)).wait_recv()
-                piece[...] = (piece[...].astype(F32) + inbox[chip, half].astype(F32)).astype(BF16)
-
-        if finished is not None:
-            finished(half)
-
-    return lambda: sweep(True)
-
-
-def mixer_kernel(
+                    for p in range(PIECES):
+                        self.copy(leg, dest, p, leg[3]).wait_send()
+
+
+def attention(
     sp_count, chips, heads, loads, later_loads,
-    q_ref, k_ref, v_ref, off_ref, doc_ref, res_ref, gain_ref, w_hbm,
-    mixed_ref, normed_ref,
-    meta_ref, doc_col, k_buf, v_buf, m_buf, acc, carry, w_buf, part, partner_in, down_in, up_in,
-    w_sem, kv_send, kv_recv, p_send, p_recv, down_send, down_recv, up_send, up_recv,
+    q_ref, k_ref, v_ref, off_ref, doc_ref,
+    meta_ref, doc_col, k_buf, v_buf, m_buf, acc, carry, kv_send, kv_recv,
 ):
     sp = lax.axis_index("sp")
     tp = lax.axis_index("tp")
@@ -155,10 +143,6 @@
     core = tp % 2
     partner = tp + 1 - 2 * core
     tok, att = q_ref.shape
-    width = res_ref.shape[1]
-    half_rows = res_ref.shape[0] // 2
-
-    w_copy = pltpu.make_async_copy(w_hbm, w_buf, w_sem)
     for j in range(1, sp_count):
         greet((lax.rem(sp + j, sp_count), tp))
     greet((sp, partner))
@@ -194,7 +178,6 @@
             for copy in kv_copies(j, sp + j):
                 copy.start()
 
-    w_copy.start()
     for copy in later_loads:
         copy.start()
 
@@ -250,10 +233,12 @@
             for copy in kv_copies(j, sp + j):
                 copy.wait_send()
 
-    w_copy.wait()
-    attended = acc[...].astype(BF16)
+    return acc[...].astype(BF16)
+
+
+def project(attended, w_buf, part, chips, half_rows, first, last):
     tile = 512
-    for n in range(width // tile):
+    for n in range(first // tile, last // tile):
         cols = slice(n * tile, (n + 1) * tile)
         product = jnp.dot(attended, w_buf[:, cols], preferred_element_type=F32).astype(BF16)
         for z in range(chips):
@@ -262,9 +247,33 @@
                     at = ((z * 2 + c) * 2 + s) * half_rows
                     part[c, z, s, :, cols] = product[at : at + half_rows]
 
+
+def mixer_kernel(
+    sp_count, chips, heads,
+    q_ref, k_ref, v_ref, off_ref, doc_ref, res_ref, gain_ref, w_hbm,
+    mixed_ref, normed_ref,
+    meta_ref, doc_col, k_buf, v_buf, m_buf, acc, carry, w_buf, part, partner_in, down_in, up_in,
+    w_sem, kv_send, kv_recv, p_send, p_recv, down_send, down_recv, up_send, up_recv,
+):
+    sp = lax.axis_index("sp")
+    tp = lax.axis_index("tp")
+    chip = tp // 2
+    core = tp % 2
+    width = res_ref.shape[1]
+    half_rows = res_ref.shape[0] // 2
+    w_copy = pltpu.make_async_copy(w_hbm, w_buf, w_sem)
+    attended = attention(
+        sp_count, chips, heads, (), (w_copy,),
+        q_ref, k_ref, v_ref, off_ref, doc_ref,
+        meta_ref, doc_col, k_buf, v_buf, m_buf, acc, carry, kv_send, kv_recv,
+    )
+    w_copy.wait()
+    project(attended, w_buf, part, chips, half_rows, 0, width)
+
     def p_copy(z):
         return remote(
-            part.at[1 - core, z], partner_in.at[z], p_send.at[z], p_recv.at[z], (sp, partner)
+            part.at[1 - core, z], partner_in.at[z], p_send.at[z, 0], p_recv.at[z, 0],
+            (sp, tp + 1 - 2 * core),
         )
 
     for z in range(chips):
@@ -272,12 +281,14 @@
     for z in range(chips):
         p_copy(z).wait_recv()
         part[core, z] = (part[core, z].astype(F32) + partner_in[z].astype(F32)).astype(BF16)
-    finish = line_reduce(
-        chips, chip, sp, tp, lambda z, p: part.at[core, z, p // 2, :, columns(p, width)], down_in, up_in,
-        (down_send, down_recv, up_send, up_recv),
-    )
-    for copy in later_loads[:1]:
-        copy.wait()
+    line = Line(
+        chips, chip, sp, tp, lambda z, p: part.at[core, z, p // 2, :, columns(p, width)],
+        down_in, up_in, (down_send, down_recv, up_send, up_recv),
+    )
+    for distance in range(chips - 1, 0, -1):
+        line.send(chip - distance, chip + distance, range(PIECES), lambda dest, p: None)
+    for p in range(PIECES):
+        line.own(p, lambda dest, p: None)
     total = part[core, chip].reshape(res_ref.shape).astype(F32)
     mixed = (res_ref[...].astype(F32) + total).astype(BF16)
     mixed_ref[...] = mixed
@@ -286,7 +297,7 @@
     normed_ref[...] = (mixed_f * scaling * gain_ref[...]).astype(BF16)
     for z in range(chips):
         p_copy(z).wait_send()
-    finish()
+    line.drain()
 
 
 def mixer_scratch(residual, queries, heads, out_weight):
@@ -315,8 +326,8 @@
         dma,
         dma((others, 3)),
         dma((others, 3)),
-        dma((chips,)),
-        dma((chips,)),
+        dma((chips, 2)),
+        dma((chips, 2)),
     ] + [dma((chips, PIECES))] * 4
 
 
@@ -324,7 +335,7 @@
     heads = offsets.shape[1]
     return pl.pallas_call(
         functools.partial(
-            mixer_kernel, lax.axis_size("sp"), lax.axis_size("tp") // 2, heads, (), ()
+            mixer_kernel, lax.axis_size("sp"), lax.axis_size("tp") // 2, heads
         ),
         out_shape=[jax.ShapeDtypeStruct(residual.shape, BF16)] * 2,
         in_specs=[VMEM_SPEC] * 7 + [ANY_SPEC],
@@ -355,9 +366,10 @@
 
 def experts_kernel(
     chips,
-    w_copies,
-    normed_ref, mixed_ref, ids_ref, group_ref, expert_ref,
+    w_copies, w_copy, res_copy, attended,
+    mixed_ref, res_ref, gain_ref, ids_ref, group_ref, expert_ref,
     out_ref,
+    w_buf, sums, sums_in, a_down_in, a_up_in, a_send, a_recv, a_sems,
     router_ref, gate, up, down, rows, y_out, part, partner_in, x_in, down_in, up_in, y_in, total,
     y_sem, rows_recv, line_send, x_send, fan_send,
     p_send, p_recv, xr_send, xr_recv, down_send, down_recv, up_send, up_recv,
@@ -371,9 +383,10 @@
     y_peer = (lax.rem(sp + 2, 4), tp)
     below, above = (sp, tp - 2), (sp, tp + 2)
     has_below, has_above = chip > 0, chip < chips - 1
-    half_rows, width = rows.shape[4:]
-
-    row_count = 2 * half_rows
+    row_count, width = res_ref.shape
+    half_rows = row_count // 2
+    half_width = width // 2
+
     slots = slot_row(ids_ref[...], tp, row_count)
     slot_iota = lax.broadcasted_iota(jnp.int32, (half_rows, row_count), 0)
 
@@ -385,59 +398,57 @@
     router_ref[...] = jnp.zeros_like(router_ref)
     router_ref[0:2, :] = group_ref[...].astype(F32)
     router_ref[2:6, :] = expert_ref[...].astype(F32)
-    own = jnp.dot(sel_own, normed_ref[...], preferred_element_type=F32).astype(BF16)
-    other = jnp.dot(sel_other, normed_ref[...], preferred_element_type=F32).astype(BF16)
-    rows[x, chip, core, y] = own
-    y_out[...] = other
-
-    y_copy = remote(
-        y_out, rows.at[x, chip, core, y], y_sem.at[0], rows_recv.at[x, chip, core, y], y_peer
-    )
-    y_copy.start()
-
-    def piece_copy(xs, z, c, s, send, device):
-        piece = rows.at[xs, z, c, s]
-        return remote(piece, piece, send, rows_recv.at[xs, z, c, s], device)
-
-    def line_piece(z, s, up_ok, down_ok, act):
+
+    def span(h):
+        return pl.ds(h * half_width, half_width + (rows.shape[5] - width) * h)
+
+    def y_copy(h):
+        return remote(
+            y_out.at[:, span(h)], rows.at[x, chip, core, y, :, span(h)], y_sem.at[5 + h],
+            rows_recv.at[x, chip, core, y, h], y_peer,
+        )
+
+    def piece_copy(xs, z, c, s, h, send, device):
+        piece = rows.at[xs, z, c, s, :, span(h)]
+        return remote(piece, piece, send, rows_recv.at[xs, z, c, s, h], device)
+
+    def line_piece(z, s, h, up_ok, down_ok, act):
         @pl.when(down_ok)
         def _():
-            act(piece_copy(x, z, core, s, line_send.at[z, s, 0], below))
+            act(piece_copy(x, z, core, s, h, line_send.at[z, s, 0, h], below))
 
         @pl.when(up_ok)
         def _():
-            act(piece_copy(x, z, core, s, line_send.at[z, s, 1], above))
-
-        act(piece_copy(x, z, core, s, x_send.at[z, s], x_peer))
-        act(piece_copy(x, z, core, s, fan_send.at[0, z, s], partner))
+            act(piece_copy(x, z, core, s, h, line_send.at[z, s, 1, h], above))
+
+        act(piece_copy(x, z, core, s, h, x_send.at[z, s, h], x_peer))
+        act(piece_copy(x, z, core, s, h, fan_send.at[0, z, s, h], partner))
 
     def begin(copy):
         copy.start()
 
-    def arrived(xs, z, c, s):
-        piece_copy(xs, z, c, s, y_sem.at[0], x_peer).wait_recv()
-
-    def own_pieces(act, wait):
-        line_piece(chip, y, has_above, has_below, act)
-        if wait:
-            arrived(x, chip, core, 1 - y)
-        line_piece(chip, 1 - y, has_above, has_below, act)
-
-    def line_pieces(distance, act, wait):
+    def arrived(xs, z, c, s, h):
+        piece_copy(xs, z, c, s, h, y_sem.at[0], x_peer).wait_recv()
+
+    def own_rest(h):
+        arrived(x, chip, core, 1 - y, h)
+        line_piece(chip, 1 - y, h, has_above, has_below, begin)
+
+    def line_pieces(distance, h, act, wait):
         for turn in range(2):
             s = y if turn == 0 else 1 - y
 
             @pl.when(chip - distance >= 0)
             def _():
                 if wait:
-                    arrived(x, chip - distance, core, s)
-                line_piece(chip - distance, s, has_above, chip < 0, act)
+                    arrived(x, chip - distance, core, s, h)
+                line_piece(chip - distance, s, h, has_above, chip < 0, act)
 
             @pl.when(chip + distance < chips)
             def _():
                 if wait:
-                    arrived(x, chip + distance, core, s)
-                line_piece(chip + distance, s, chip < 0, has_below, act)
+                    arrived(x, chip + distance, core, s, h)
+                line_piece(chip + distance, s, h, chip < 0, has_below, act)
 
     def at_distance(distance, body):
         if distance == 0:
@@ -452,12 +463,78 @@
         def _():
             body(chip + distance)
 
-    def cross(z, act, wait):
+    def cross(z, h, act, wait):
         for turn in range(2):
             s = y if turn == 0 else 1 - y
             if wait:
-                arrived(1 - x, z, core, s)
-            act(piece_copy(1 - x, z, core, s, fan_send.at[1, z, s], partner))
+                arrived(1 - x, z, core, s, h)
+            act(piece_copy(1 - x, z, core, s, h, fan_send.at[1, z, s, h], partner))
+
+    def a_copy(z, h):
+        cols = columns(h, width)
+        return remote(
+            sums.at[1 - core, z, :, :, cols], sums_in.at[z, :, :, cols], a_send.at[z, h],
+            a_recv.at[z, h], partner,
+        )
+
+    w_copy.wait()
+    for h in range(2):
+        project(attended, w_buf, sums, chips, half_rows, h * half_width, (h + 1) * half_width)
+        for z in range(chips):
+            a_copy(z, h).start()
+
+    def fold(dest, p):
+        if p < 2:
+            cols = columns(p, width)
+            a_copy(dest, p).wait_recv()
+            sums[core, dest, :, :, cols] = (
+                sums[core, dest, :, :, cols].astype(F32) + sums_in[dest, :, :, cols].astype(F32)
+            ).astype(BF16)
+
+    mix = Line(
+        chips, chip, sp, tp, lambda z, p: sums.at[core, z, p // 2, :, columns(p, width)],
+        a_down_in, a_up_in, a_sems,
+    )
+
+    def mix_turn(distance, h):
+        mix.send(chip - distance, chip + distance, (h, 2 + h), fold)
+
+    squares = []
+
+    def settle(h):
+        for p in (h, 2 + h):
+            mix.own(p, fold)
+        cols = columns(h, width)
+        added = sums[core, chip, :, :, cols].reshape(row_count, half_width).astype(F32)
+        mixed = (res_ref[:, cols].astype(F32) + added).astype(BF16)
+        mixed_ref[:, cols] = mixed
+        mixed_f = mixed.astype(F32)
+        squares.append(jnp.sum(mixed_f * mixed_f, axis=1, keepdims=True))
+        scaled = (mixed_f * gain_ref[:, cols]).astype(BF16)
+
+        def put(group_sel, target):
+            target[:, pl.ds(h * half_width, half_width)] = jnp.dot(
+                group_sel, scaled, preferred_element_type=F32
+            ).astype(BF16)
+
+        own_rows = rows.at[x, chip, core, y]
+        put(sel_other, y_out)
+        put(sel_own, own_rows)
+        if h == 1:
+            factor = lax.rsqrt((squares[0] + squares[1]) * (1.0 / width) + 1e-06)
+            high = factor.astype(BF16).astype(F32)
+            middle = (factor - high).astype(BF16).astype(F32)
+            low = factor - high - middle
+            lane = lax.broadcasted_iota(jnp.int32, (row_count, 128), 1)
+            terms = jnp.where(
+                lane == 0, high, jnp.where(lane == 1, middle, jnp.where(lane == 2, low, 0.0))
+            ).astype(BF16)
+            for group_sel, target in ((sel_other, y_out), (sel_own, own_rows)):
+                target[:, pl.ds(width, 128)] = jnp.dot(
+                    group_sel, terms, preferred_element_type=F32
+                ).astype(BF16)
+        y_copy(h).start()
+        line_piece(chip, y, h, has_above, has_below, begin)
 
     def p_copy(z):
         return remote(part.at[z, 1 - core], partner_in.at[z], p_send.at[z], p_recv.at[z], partner)
@@ -476,18 +553,22 @@
     expert_sign = signed(2 + sp, 2 + sp + 1 - 2 * x)
 
     def expert(z):
-        for xs in range(2):
-            for s in range(2):
-                arrived(xs, z, 1 - core, s)
-        block = rows[:, z].reshape(8 * half_rows, width)
+        for h in range(2):
+            for xs in range(2):
+                for s in range(2):
+                    arrived(xs, z, 1 - core, s, h)
+        block = rows[:, z, :, :, :, :width].reshape(8 * half_rows, width)
+        terms = rows[:, z, :, :, :, width:].reshape(8 * half_rows, rows.shape[5] - width)
+        factor = jnp.sum(terms.astype(F32), axis=1, keepdims=True)
         logits = lax.dot_general(
             block, router_ref[...].astype(BF16), (((1,), (1,)), ((), ())), preferred_element_type=F32
         )
+        logits = logits * factor
         route = jax.nn.sigmoid(
             jnp.sum(logits * group_sign, axis=1, keepdims=True)
         ) * jax.nn.sigmoid(jnp.sum(logits * expert_sign, axis=1, keepdims=True))
-        gated = jnp.dot(block, gate[...], preferred_element_type=F32)
-        raised = jnp.dot(block, up[...], preferred_element_type=F32)
+        gated = jnp.dot(block, gate[...], preferred_element_type=F32) * factor
+        raised = jnp.dot(block, up[...], preferred_element_type=F32) * factor
         hidden = (jax.nn.silu(gated) * raised).astype(BF16)
         tile = 1024
         for n in range(width // tile):
@@ -539,11 +620,31 @@
             )
             total[:, cols] = mixed_ref[:, cols].astype(F32) + sums
 
-    own_pieces(begin, True)
+    for distance in range(chips - 1, 0, -1):
+        mix_turn(distance, 0)
+    mix_turn(chips - 1, 1)
+    res_copy.wait()
+    settle(0)
+    for distance in range(chips - 2, 0, -1):
+        mix_turn(distance, 1)
+        if distance == chips - 2:
+            own_rest(0)
+    line_pieces(1, 0, begin, True)
+    settle(1)
+
+    def cross_all(distance, h):
+        at_distance(distance, lambda z: cross(z, h, begin, True))
+
     for distance in range(1, chips + 1):
+        if distance + 1 < chips:
+            line_pieces(distance + 1, 0, begin, True)
+        if distance == 1:
+            own_rest(1)
+            cross_all(0, 0)
         if distance < chips:
-            line_pieces(distance, begin, True)
-        at_distance(distance - 1, lambda z: cross(z, begin, True))
+            line_pieces(distance, 1, begin, True)
+            cross_all(distance, 0)
+        cross_all(distance - 1, 1)
         if distance == 1:
             for copy in w_copies:
                 copy.wait()
@@ -553,34 +654,45 @@
     at_distance(chips - 1, join_cores)
     for s in halves:
         xr_copy(chip, s).start()
-    finish = line_reduce(
+    back = Line(
         chips, chip, sp, tp,
         lambda z, p: part.at[z, core, x, halves[p // 2], :, columns(p, width)],
-        down_in, up_in, (down_send, down_recv, up_send, up_recv), join_x, finished, True,
-    )
+        down_in, up_in, (down_send, down_recv, up_send, up_recv),
+    )
+    for turn in range(1, 2 * chips - 2):
+        back.send(2 * (chips - 1) - turn - chip, turn - chip, range(PIECES), join_x)
+    for p in range(PIECES):
+        back.own(p, join_x)
+        finished(p)
     for n in range(2):
         cols = columns(n, width)
         back_copy(n).wait_recv()
-        sums = lax.dot_general(
+        returned = lax.dot_general(
             sel_other, y_in[:, cols], (((0,), (0,)), ((), ())), preferred_element_type=F32
         )
-        out_ref[:, cols] = (total[:, cols] + sums).astype(BF16)
+        out_ref[:, cols] = (total[:, cols] + returned).astype(BF16)
 
     def end(copy):
         copy.wait_send()
 
     for n in range(2):
         back_copy(n).wait_send()
-    y_copy.wait_send()
-    own_pieces(end, False)
-    for distance in range(chips):
-        if distance:
-            line_pieces(distance, end, False)
-        at_distance(distance, lambda z: cross(z, end, False))
-        at_distance(distance, lambda z: end(p_copy(z)))
+    for h in range(2):
+        y_copy(h).wait_send()
+        for s in (y, 1 - y):
+            line_piece(chip, s, h, has_above, has_below, end)
+        for distance in range(chips):
+            if distance:
+                line_pieces(distance, h, end, False)
+            at_distance(distance, lambda z: cross(z, h, end, False))
+        for z in range(chips):
+            end(a_copy(z, h))
+    for z in range(chips):
+        end(p_copy(z))
         for s in range(2):
-            at_distance(distance, lambda z: end(xr_copy(z, s)))
-    finish()
+            end(xr_copy(z, s))
+    mix.drain()
+    back.drain()
 
 
 def layer_kernel(
@@ -588,7 +700,7 @@
     q_hbm, k_hbm, v_hbm, res_hbm, w_hbm, gate_hbm, up_hbm, down_hbm,
     off_ref, doc_ref, gain_ref, ids_ref, group_ref, expert_ref,
     out_ref,
-    q_ref, k_ref, v_ref, res_ref, mixed_ref, normed_ref, load_sem, weight_sem, router_ref,
+    q_ref, k_ref, v_ref, res_ref, mixed_ref, load_sem, weight_sem, router_ref,
     gate, up, down,
     *scratch,
 ):
@@ -604,13 +716,21 @@
     ]
     for copy in loads[:3]:
         copy.start()
-    mixer_kernel(
-        sp_count, chips, heads, loads[:3], loads[3:] + weights,
-        q_ref, k_ref, v_ref, off_ref, doc_ref, res_ref, gain_ref, w_hbm,
-        mixed_ref, normed_ref, *scratch[:mixer_count],
+    (
+        meta_ref, doc_col, k_buf, v_buf, m_buf, acc, carry, w_buf, sums, sums_in, a_down_in, a_up_in,
+        w_sem, kv_send, kv_recv, a_send, a_recv,
+    ) = scratch[: mixer_count - 4]
+    a_sems = scratch[mixer_count - 4 : mixer_count]
+    w_copy = pltpu.make_async_copy(w_hbm, w_buf, w_sem)
+    attended = attention(
+        sp_count, chips, heads, loads[:3], [w_copy, loads[3]] + weights,
+        q_ref, k_ref, v_ref, off_ref, doc_ref,
+        meta_ref, doc_col, k_buf, v_buf, m_buf, acc, carry, kv_send, kv_recv,
     )
     experts_kernel(
-        chips, weights, normed_ref, mixed_ref, ids_ref, group_ref, expert_ref, out_ref,
+        chips, weights, w_copy, loads[3], attended,
+        mixed_ref, res_ref, gain_ref, ids_ref, group_ref, expert_ref, out_ref,
+        w_buf, sums, sums_in, a_down_in, a_up_in, a_send, a_recv, a_sems,
         router_ref, gate, up, down, *scratch[mixer_count:],
     )
 
@@ -641,7 +761,6 @@
             pltpu.VMEM(values.shape, BF16),
             pltpu.VMEM((rows, width), BF16),
             pltpu.VMEM((rows, width), BF16),
-            pltpu.VMEM((rows, width), BF16),
             dma((4,)),
             dma((3,)),
             pltpu.VMEM((8, width), F32),
@@ -651,8 +770,8 @@
         ]
         + mixer_parts
         + [
-            pltpu.VMEM((2, chips, 2, 2, half_rows, width), BF16),
-            pltpu.VMEM((half_rows, width), BF16),
+            pltpu.VMEM((2, chips, 2, 2, half_rows, width + 128), BF16),
+            pltpu.VMEM((half_rows, width + 128), BF16),
             pltpu.VMEM((chips, 2, 2, 2, half_rows, width), BF16),
             pltpu.VMEM((chips, 2, 2, half_rows, width), BF16),
             pltpu.VMEM(half, BF16),
@@ -660,11 +779,11 @@
             pltpu.VMEM(quarter, BF16),
             pltpu.VMEM((half_rows, width), BF16),
             pltpu.VMEM((rows, width), F32),
-            dma((5,)),
+            dma((7,)),
+            dma((2, chips, 2, 2, 2)),
+            dma((chips, 2, 2, 2)),
+            dma((chips, 2, 2)),
             dma((2, chips, 2, 2)),
-            dma((chips, 2, 2)),
-            dma((chips, 2)),
-            dma((2, chips, 2)),
             dma((chips,)),
             dma((chips,)),
             dma((chips, 2)),

time: 109 us -> 109 us (level)
  no operation moved by 1% of the time
where the time goes in v2:
time: 109 us
  Pallas kernels  107 us (98%)
  local copies, waits for them, and re-layouts  1.67 us (2%)
    pallas_call x1, Pallas kernels, pair_layer(): pl.pallas_call(functools.partial(layer_kernel, lax.axis_size('sp'), chips...  107 us

profile of v2, /device:TPU:0, one launch (start us, length us, event | category | flops | bytes accessed | tf_op | source)
XLA Modules:
  0.0 109.0 jit_solution(8769708433918804382)
XLA Ops:
  0.0 107.4 %layer.1 = bf16[32,4096]{1,0:T(8,128)(2,1)} custom-call(bf16[256,256]{1,0:T(8,128)(2,1)} %q_hbm.1, bf16[256,256]{1,0:T(8,128)(2,1)} %k_hbm.1, bf16[256,256]{1,0:T(8,128)(2,1)} %v_hbm.1, bf16[32,4096]{1,0:T(8,128)(2,1)} %res_hbm.1, bf16[256,4096]{1,0:T(8,128)(2,1)} %w_hbm.1, bf16[1,4096,512]{2,1,0:T(8,128)(2,1)} %gate_hbm.1, bf16[1,4096,512]{2,1,0:T(8,128)(2,1)} %up_hbm.1, ...), custom_call_target="tpu_custom_call" | custom-call | tf_op jit(solution)/shard_map/layer/pallas_call | solution.py:751
  107.4 1.7 %copy.16 = bf16[32,4096]{1,0:T(8,128)(2,1)} copy(bf16[32,4096]{1,0:T(8,128)(2,1)} %layer.1) | data formatting | bytes 524288

commit v3 on v2

--- a/solution.py
+++ b/solution.py
@@ -226,14 +226,16 @@
         return unused
 
     lax.fori_loop(1, sp_count, earlier, 0)
-    for j in range(1, sp_count):
-
-        @pl.when(sp + j < sp_count)
-        def _():
-            for copy in kv_copies(j, sp + j):
-                copy.wait_send()
-
-    return acc[...].astype(BF16)
+
+    def drain():
+        for j in range(1, sp_count):
+
+            @pl.when(sp + j < sp_count)
+            def _():
+                for copy in kv_copies(j, sp + j):
+                    copy.wait_send()
+
+    return acc[...].astype(BF16), drain
 
 
 def project(attended, w_buf, part, chips, half_rows, first, last):
@@ -262,7 +264,7 @@
     width = res_ref.shape[1]
     half_rows = res_ref.shape[0] // 2
     w_copy = pltpu.make_async_copy(w_hbm, w_buf, w_sem)
-    attended = attention(
+    attended, drain_kv = attention(
         sp_count, chips, heads, (), (w_copy,),
         q_ref, k_ref, v_ref, off_ref, doc_ref,
         meta_ref, doc_col, k_buf, v_buf, m_buf, acc, carry, kv_send, kv_recv,
@@ -298,6 +300,7 @@
     for z in range(chips):
         p_copy(z).wait_send()
     line.drain()
+    drain_kv()
 
 
 def mixer_scratch(residual, queries, heads, out_weight):
@@ -400,7 +403,7 @@
     router_ref[2:6, :] = expert_ref[...].astype(F32)
 
     def span(h):
-        return pl.ds(h * half_width, half_width + (rows.shape[5] - width) * h)
+        return columns(h, width)
 
     def y_copy(h):
         return remote(
@@ -430,13 +433,13 @@
     def arrived(xs, z, c, s, h):
         piece_copy(xs, z, c, s, h, y_sem.at[0], x_peer).wait_recv()
 
-    def own_rest(h):
-        arrived(x, chip, core, 1 - y, h)
-        line_piece(chip, 1 - y, h, has_above, has_below, begin)
-
-    def line_pieces(distance, h, act, wait):
-        for turn in range(2):
-            s = y if turn == 0 else 1 - y
+    def own_rest(s):
+        for h in range(2):
+            arrived(x, chip, core, s, h)
+            line_piece(chip, s, h, has_above, has_below, begin)
+
+    def line_pieces(distance, s, act, wait):
+        for h in range(2):
 
             @pl.when(chip - distance >= 0)
             def _():
@@ -463,9 +466,8 @@
         def _():
             body(chip + distance)
 
-    def cross(z, h, act, wait):
-        for turn in range(2):
-            s = y if turn == 0 else 1 - y
+    def cross(z, s, act, wait):
+        for h in range(2):
             if wait:
                 arrived(1 - x, z, core, s, h)
             act(piece_copy(1 - x, z, core, s, h, fan_send.at[1, z, s, h], partner))
@@ -496,45 +498,25 @@
         a_down_in, a_up_in, a_sems,
     )
 
-    def mix_turn(distance, h):
-        mix.send(chip - distance, chip + distance, (h, 2 + h), fold)
-
-    squares = []
-
-    def settle(h):
-        for p in (h, 2 + h):
+    def settle():
+        for p in range(PIECES):
             mix.own(p, fold)
-        cols = columns(h, width)
-        added = sums[core, chip, :, :, cols].reshape(row_count, half_width).astype(F32)
-        mixed = (res_ref[:, cols].astype(F32) + added).astype(BF16)
-        mixed_ref[:, cols] = mixed
+        added = sums[core, chip].reshape(row_count, width).astype(F32)
+        mixed = (res_ref[...].astype(F32) + added).astype(BF16)
+        mixed_ref[...] = mixed
         mixed_f = mixed.astype(F32)
-        squares.append(jnp.sum(mixed_f * mixed_f, axis=1, keepdims=True))
-        scaled = (mixed_f * gain_ref[:, cols]).astype(BF16)
-
-        def put(group_sel, target):
-            target[:, pl.ds(h * half_width, half_width)] = jnp.dot(
-                group_sel, scaled, preferred_element_type=F32
+        scaling = lax.rsqrt(jnp.mean(mixed_f * mixed_f, axis=1, keepdims=True) + 1e-06)
+        normed = (mixed_f * scaling * gain_ref[...]).astype(BF16)
+        for h in range(2):
+            cols = slice(h * half_width, (h + 1) * half_width)
+            y_out[:, cols] = jnp.dot(
+                sel_other, normed[:, cols], preferred_element_type=F32
             ).astype(BF16)
-
-        own_rows = rows.at[x, chip, core, y]
-        put(sel_other, y_out)
-        put(sel_own, own_rows)
-        if h == 1:
-            factor = lax.rsqrt((squares[0] + squares[1]) * (1.0 / width) + 1e-06)
-            high = factor.astype(BF16).astype(F32)
-            middle = (factor - high).astype(BF16).astype(F32)
-            low = factor - high - middle
-            lane = lax.broadcasted_iota(jnp.int32, (row_count, 128), 1)
-            terms = jnp.where(
-                lane == 0, high, jnp.where(lane == 1, middle, jnp.where(lane == 2, low, 0.0))
+            y_copy(h).start()
+            rows[x, chip, core, y, :, cols] = jnp.dot(
+                sel_own, normed[:, cols], preferred_element_type=F32
             ).astype(BF16)
-            for group_sel, target in ((sel_other, y_out), (sel_own, own_rows)):
-                target[:, pl.ds(width, 128)] = jnp.dot(
-                    group_sel, terms, preferred_element_type=F32
-                ).astype(BF16)
-        y_copy(h).start()
-        line_piece(chip, y, h, has_above, has_below, begin)
+            line_piece(chip, y, h, has_above, has_below, begin)
 
     def p_copy(z):
         return remote(part.at[z, 1 - core], partner_in.at[z], p_send.at[z], p_recv.at[z], partner)
@@ -557,18 +539,15 @@
             for xs in range(2):
                 for s in range(2):
                     arrived(xs, z, 1 - core, s, h)
-        block = rows[:, z, :, :, :, :width].reshape(8 * half_rows, width)
-        terms = rows[:, z, :, :, :, width:].reshape(8 * half_rows, rows.shape[5] - width)
-        factor = jnp.sum(terms.astype(F32), axis=1, keepdims=True)
+        block = rows[:, z].reshape(8 * half_rows, width)
         logits = lax.dot_general(
             block, router_ref[...].astype(BF16), (((1,), (1,)), ((), ())), preferred_element_type=F32
         )
-        logits = logits * factor
         route = jax.nn.sigmoid(
             jnp.sum(logits * group_sign, axis=1, keepdims=True)
         ) * jax.nn.sigmoid(jnp.sum(logits * expert_sign, axis=1, keepdims=True))
-        gated = jnp.dot(block, gate[...], preferred_element_type=F32) * factor
-        raised = jnp.dot(block, up[...], preferred_element_type=F32) * factor
+        gated = jnp.dot(block, gate[...], preferred_element_type=F32)
+        raised = jnp.dot(block, up[...], preferred_element_type=F32)
         hidden = (jax.nn.silu(gated) * raised).astype(BF16)
         tile = 1024
         for n in range(width // tile):
@@ -584,6 +563,9 @@
 
     halves = (1 - y, y)
 
+    def send_x(z, s):
+        xr_copy(z, s).start()
+
     def join_cores(z, send=True):
         p_copy(z).wait_recv()
         for xs in (1 - x, x):
@@ -621,46 +603,90 @@
             total[:, cols] = mixed_ref[:, cols].astype(F32) + sums
 
     for distance in range(chips - 1, 0, -1):
-        mix_turn(distance, 0)
-    mix_turn(chips - 1, 1)
+        mix.send(chip - distance, chip + distance, range(PIECES), fold)
     res_copy.wait()
-    settle(0)
-    for distance in range(chips - 2, 0, -1):
-        mix_turn(distance, 1)
-        if distance == chips - 2:
-            own_rest(0)
+
+    def cross_all(distance, s):
+        at_distance(distance, lambda z: cross(z, s, begin, True))
+
+    @pl.when(y == 0)
+    def _():
+        settle()
+
+    @pl.when(y == 1)
+    def _():
+        own_rest(0)
+        settle()
+
     line_pieces(1, 0, begin, True)
-    settle(1)
-
-    def cross_all(distance, h):
-        at_distance(distance, lambda z: cross(z, h, begin, True))
-
-    for distance in range(1, chips + 1):
-        if distance + 1 < chips:
-            line_pieces(distance + 1, 0, begin, True)
-        if distance == 1:
-            own_rest(1)
-            cross_all(0, 0)
-        if distance < chips:
-            line_pieces(distance, 1, begin, True)
-            cross_all(distance, 0)
-        cross_all(distance - 1, 1)
-        if distance == 1:
-            for copy in w_copies:
-                copy.wait()
-        at_distance(distance - 1, expert)
-        if distance > 1:
-            at_distance(distance - 2, lambda z: join_cores(z, distance > 2))
-    at_distance(chips - 1, join_cores)
-    for s in halves:
-        xr_copy(chip, s).start()
+
+    @pl.when(y == 1)
+    def _():
+        line_pieces(1, 1, begin, True)
+
+    line_pieces(2, 0, begin, True)
+
+    @pl.when(y == 0)
+    def _():
+        own_rest(1)
+        line_pieces(1, 1, begin, True)
+
+    cross_all(0, 0)
+    cross_all(1, 0)
+    cross_all(0, 1)
+    for copy in w_copies:
+        copy.wait()
+    is_end = (chip == 0) | (chip == chips - 1)
+
+    at_distance(0, expert)
+    line_pieces(2, 1, begin, True)
+    cross_all(1, 1)
+    at_distance(1, expert)
+    at_distance(0, lambda z: join_cores(z, False))
+    for s in range(2):
+        line_pieces(3, s, begin, True)
+        cross_all(2, s)
+    at_distance(1, join_cores)
+    at_distance(2, expert)
+
+    @pl.when(is_end)
+    def _():
+        send_x(chip, 1 - y)
+
+    for s in range(2):
+        cross_all(3, s)
+    at_distance(2, lambda z: join_cores(z, False))
+
+    @pl.when(jnp.logical_not(is_end))
+    def _():
+        for s in halves:
+            at_distance(2, lambda z: send_x(z, s))
+        send_x(chip, 1 - y)
+
+    at_distance(3, expert)
+    at_distance(3, join_cores)
+
+    @pl.when(is_end)
+    def _():
+        for s in halves:
+            at_distance(2, lambda z: send_x(z, s))
+
+    send_x(chip, y)
     back = Line(
         chips, chip, sp, tp,
         lambda z, p: part.at[z, core, x, halves[p // 2], :, columns(p, width)],
         down_in, up_in, (down_send, down_recv, up_send, up_recv),
     )
-    for turn in range(1, 2 * chips - 2):
-        back.send(2 * (chips - 1) - turn - chip, turn - chip, range(PIECES), join_x)
+    def back_turn(distance, mine):
+        back.send(
+            jnp.where(mine, chip - distance, -1), jnp.where(mine, chip + distance, chips),
+            range(PIECES), join_x,
+        )
+
+    back_turn(1, is_end)
+    for distance in range(chips - 1, 1, -1):
+        back_turn(distance, True)
+    back_turn(1, jnp.logical_not(is_end))
     for p in range(PIECES):
         back.own(p, join_x)
         finished(p)
@@ -679,14 +705,15 @@
         back_copy(n).wait_send()
     for h in range(2):
         y_copy(h).wait_send()
-        for s in (y, 1 - y):
+        for s in range(2):
             line_piece(chip, s, h, has_above, has_below, end)
+        for z in range(chips):
+            end(a_copy(z, h))
+    for s in range(2):
         for distance in range(chips):
             if distance:
-                line_pieces(distance, h, end, False)
-            at_distance(distance, lambda z: cross(z, h, end, False))
-        for z in range(chips):
-            end(a_copy(z, h))
+                line_pieces(distance, s, end, False)
+            at_distance(distance, lambda z: cross(z, s, end, False))
     for z in range(chips):
         end(p_copy(z))
         for s in range(2):
@@ -722,7 +749,7 @@
     ) = scratch[: mixer_count - 4]
     a_sems = scratch[mixer_count - 4 : mixer_count]
     w_copy = pltpu.make_async_copy(w_hbm, w_buf, w_sem)
-    attended = attention(
+    attended, drain_kv = attention(
         sp_count, chips, heads, loads[:3], [w_copy, loads[3]] + weights,
         q_ref, k_ref, v_ref, off_ref, doc_ref,
         meta_ref, doc_col, k_buf, v_buf, m_buf, acc, carry, kv_send, kv_recv,
@@ -733,6 +760,7 @@
         w_buf, sums, sums_in, a_down_in, a_up_in, a_send, a_recv, a_sems,
         router_ref, gate, up, down, *scratch[mixer_count:],
     )
+    drain_kv()
 
 
 def pair_layer(
@@ -770,8 +798,8 @@
         ]
         + mixer_parts
         + [
-            pltpu.VMEM((2, chips, 2, 2, half_rows, width + 128), BF16),
-            pltpu.VMEM((half_rows, width + 128), BF16),
+            pltpu.VMEM((2, chips, 2, 2, half_rows, width), BF16),
+            pltpu.VMEM((half_rows, width), BF16),
             pltpu.VMEM((chips, 2, 2, 2, half_rows, width), BF16),
             pltpu.VMEM((chips, 2, 2, half_rows, width), BF16),
             pltpu.VMEM(half, BF16),

time: 109 us -> 103 us (0.945)
  Pallas kernels: 107 us -> 101 us
    pallas_call x1, Pallas kernels: 107 us -> 101 us  [pair_layer(): pl.pallas_call(functools.partial(layer_kernel, lax.axis_size('sp'), chips...]
where the time goes in v3:
time: 103 us
  Pallas kernels  101 us (98%)
  local copies, waits for them, and re-layouts  1.67 us (2%)
    pallas_call x1, Pallas kernels, pair_layer(): pl.pallas_call(functools.partial(layer_kernel, lax.axis_size('sp'), chips...  101 us

profile of v3, /device:TPU:0, one launch (start us, length us, event | category | flops | bytes accessed | tf_op | source)
XLA Modules:
  0.0 102.8 jit_solution(6394454748526393888)
XLA Ops:
  0.0 101.1 %layer.1 = bf16[32,4096]{1,0:T(8,128)(2,1)} custom-call(bf16[256,256]{1,0:T(8,128)(2,1)} %q_hbm.1, bf16[256,256]{1,0:T(8,128)(2,1)} %k_hbm.1, bf16[256,256]{1,0:T(8,128)(2,1)} %v_hbm.1, bf16[32,4096]{1,0:T(8,128)(2,1)} %res_hbm.1, bf16[256,4096]{1,0:T(8,128)(2,1)} %w_hbm.1, bf16[1,4096,512]{2,1,0:T(8,128)(2,1)} %gate_hbm.1, bf16[1,4096,512]{2,1,0:T(8,128)(2,1)} %up_hbm.1, ...), custom_call_target="tpu_custom_call" | custom-call | tf_op jit(solution)/shard_map/layer/pallas_call | solution.py:779
  101.2 1.7 %copy.16 = bf16[32,4096]{1,0:T(8,128)(2,1)} copy(bf16[32,4096]{1,0:T(8,128)(2,1)} %layer.1) | data formatting | bytes 524288

commit v4 on v3

--- a/solution.py
+++ b/solution.py
@@ -82,8 +82,8 @@
 
 
 class Line:
-    def __init__(self, chips, chip, sp, tp, block, down_in, up_in, sems):
-        self.chips, self.chip, self.me, self.block = chips, chip, (sp, tp), block
+    def __init__(self, chips, chip, sp, tp, whole, block, down_in, up_in, sems):
+        self.chips, self.chip, self.whole, self.block = chips, chip, whole, block
         down_send, down_recv, up_send, up_recv = sems
         self.legs = (
             (down_in, down_send, down_recv, (sp, tp - 2), chip < chips - 1),
@@ -93,7 +93,7 @@
     def copy(self, leg, dest, p, device):
         inbox, send, recv = leg[:3]
         return remote(
-            self.block(dest, p), inbox.at[dest, p], send.at[dest, p], recv.at[dest, p], device
+            self.block(dest, p), inbox.at[dest, p], send.at[dest], recv.at[dest, p], device
         )
 
     def gather(self, leg, dest, p, device):
@@ -128,12 +128,14 @@
 
                 @pl.when(sent)
                 def _():
-                    for p in range(PIECES):
-                        self.copy(leg, dest, p, leg[3]).wait_send()
+                    chunk = self.whole(dest)
+                    remote(
+                        chunk, chunk, leg[1].at[dest], leg[2].at[dest, 0], leg[3]
+                    ).wait_send()
 
 
 def attention(
-    sp_count, chips, heads, loads, later_loads,
+    sp_count, chips, heads, relay, loads, later_loads,
     q_ref, k_ref, v_ref, off_ref, doc_ref,
     meta_ref, doc_col, k_buf, v_buf, m_buf, acc, carry, kv_send, kv_recv,
 ):
@@ -171,12 +173,28 @@
             for n, (src, buf) in enumerate(((k_ref, k_buf), (v_ref, v_buf), (meta_ref, m_buf)))
         ]
 
-    for j in range(1, sp_count):
-
-        @pl.when(sp + j < sp_count)
-        def _():
-            for copy in kv_copies(j, sp + j):
-                copy.start()
+    def sends(act):
+        for j in range(1, sp_count):
+            keys, *others = kv_copies(j, sp + j)
+            direct = sp + j < sp_count
+
+            @pl.when(direct & (sp + j != sp_count - 1 - sp) if relay else direct)
+            def _():
+                act(keys)
+
+            @pl.when(direct)
+            def _():
+                for copy in others:
+                    act(copy)
+
+    def relayed():
+        slot = 2 * x_peer - sp_count
+        return remote(
+            k_buf.at[1], k_buf.at[slot], kv_send.at[2, 0], kv_recv.at[slot, 0], (x_peer, tp)
+        )
+
+    x_peer = sp + 1 - 2 * (sp % 2)
+    sends(lambda copy: copy.start())
 
     for copy in later_loads:
         copy.start()
@@ -216,10 +234,23 @@
 
     attend_block(k_ref[...], v_ref[...], meta_ref[...], True)
 
+    if relay:
+
+        @pl.when(sp >= 2)
+        def _():
+            kv_copies(2, sp)[0].wait_recv()
+            relayed().start()
+
     def earlier(j, unused):
         @pl.when(sp - j >= 0)
         def _():
-            for copy in kv_copies(j, sp):
+            keys, *others = kv_copies(j, sp)
+
+            @pl.when((sp < 2) | (j != 2) if relay else True)
+            def _():
+                keys.wait_recv()
+
+            for copy in others:
                 copy.wait_recv()
             attend_block(k_buf[j - 1], v_buf[j - 1], m_buf[j - 1], False)
 
@@ -228,12 +259,12 @@
     lax.fori_loop(1, sp_count, earlier, 0)
 
     def drain():
-        for j in range(1, sp_count):
-
-            @pl.when(sp + j < sp_count)
+        sends(lambda copy: copy.wait_send())
+        if relay:
+
+            @pl.when(sp >= 2)
             def _():
-                for copy in kv_copies(j, sp + j):
-                    copy.wait_send()
+                relayed().wait_send()
 
     return acc[...].astype(BF16), drain
 
@@ -265,7 +296,7 @@
     half_rows = res_ref.shape[0] // 2
     w_copy = pltpu.make_async_copy(w_hbm, w_buf, w_sem)
     attended, drain_kv = attention(
-        sp_count, chips, heads, (), (w_copy,),
+        sp_count, chips, heads, False, (), (w_copy,),
         q_ref, k_ref, v_ref, off_ref, doc_ref,
         meta_ref, doc_col, k_buf, v_buf, m_buf, acc, carry, kv_send, kv_recv,
     )
@@ -274,7 +305,7 @@
 
     def p_copy(z):
         return remote(
-            part.at[1 - core, z], partner_in.at[z], p_send.at[z, 0], p_recv.at[z, 0],
+            part.at[1 - core, z], partner_in.at[z], p_send.at[z], p_recv.at[z, 0],
             (sp, tp + 1 - 2 * core),
         )
 
@@ -284,7 +315,8 @@
         p_copy(z).wait_recv()
         part[core, z] = (part[core, z].astype(F32) + partner_in[z].astype(F32)).astype(BF16)
     line = Line(
-        chips, chip, sp, tp, lambda z, p: part.at[core, z, p // 2, :, columns(p, width)],
+        chips, chip, sp, tp, lambda z: part.at[core, z],
+        lambda z, p: part.at[core, z, p // 2, :, columns(p, width)],
         down_in, up_in, (down_send, down_recv, up_send, up_recv),
     )
     for distance in range(chips - 1, 0, -1):
@@ -329,9 +361,9 @@
         dma,
         dma((others, 3)),
         dma((others, 3)),
+        dma((chips,)),
         dma((chips, 2)),
-        dma((chips, 2)),
-    ] + [dma((chips, PIECES))] * 4
+    ] + [dma((chips,)), dma((chips, PIECES))] * 2
 
 
 def mixer(residual, queries, keys, values, offsets, docs, out_weight, gain):
@@ -369,13 +401,12 @@
 
 def experts_kernel(
     chips,
-    w_copies, w_copy, res_copy, attended,
+    w_copies, w_copy, res_copy, attended, drain_kv,
     mixed_ref, res_ref, gain_ref, ids_ref, group_ref, expert_ref,
     out_ref,
     w_buf, sums, sums_in, a_down_in, a_up_in, a_send, a_recv, a_sems,
     router_ref, gate, up, down, rows, y_out, part, partner_in, x_in, down_in, up_in, y_in, total,
-    y_sem, rows_recv, line_send, x_send, fan_send,
-    p_send, p_recv, xr_send, xr_recv, down_send, down_recv, up_send, up_recv,
+    out_buf, out_sem, y_sem, rows_recv, fan_recv, line_send, bulk, p_recv, xr_recv,
 ):
     sp = lax.axis_index("sp")
     tp = lax.axis_index("tp")
@@ -408,34 +439,38 @@
     def y_copy(h):
         return remote(
             y_out.at[:, span(h)], rows.at[x, chip, core, y, :, span(h)], y_sem.at[5 + h],
-            rows_recv.at[x, chip, core, y, h], y_peer,
-        )
-
-    def piece_copy(xs, z, c, s, h, send, device):
-        piece = rows.at[xs, z, c, s, :, span(h)]
-        return remote(piece, piece, send, rows_recv.at[xs, z, c, s, h], device)
+            rows_recv.at[x, chip, y, h], y_peer,
+        )
+
+    def piece_copy(xs, z, s, h, send, device):
+        piece = rows.at[xs, z, core, s, :, span(h)]
+        return remote(piece, piece, send, rows_recv.at[xs, z, s, h], device)
+
+    def fan_copy(xs, z, s, h):
+        piece = rows.at[xs, z, core, s, :, span(h)]
+        return remote(piece, piece, bulk.at[0], fan_recv.at[z], partner)
 
     def line_piece(z, s, h, up_ok, down_ok, act):
         @pl.when(down_ok)
         def _():
-            act(piece_copy(x, z, core, s, h, line_send.at[z, s, 0, h], below))
+            act(piece_copy(x, z, s, h, line_send.at[z, 0], below))
 
         @pl.when(up_ok)
         def _():
-            act(piece_copy(x, z, core, s, h, line_send.at[z, s, 1, h], above))
-
-        act(piece_copy(x, z, core, s, h, x_send.at[z, s, h], x_peer))
-        act(piece_copy(x, z, core, s, h, fan_send.at[0, z, s, h], partner))
+            act(piece_copy(x, z, s, h, line_send.at[z, 1], above))
+
+        act(piece_copy(x, z, s, h, bulk.at[1], x_peer))
+        act(fan_copy(x, z, s, h))
 
     def begin(copy):
         copy.start()
 
-    def arrived(xs, z, c, s, h):
-        piece_copy(xs, z, c, s, h, y_sem.at[0], x_peer).wait_recv()
+    def arrived(xs, z, s, h):
+        piece_copy(xs, z, s, h, y_sem.at[0], x_peer).wait_recv()
 
     def own_rest(s):
         for h in range(2):
-            arrived(x, chip, core, s, h)
+            arrived(x, chip, s, h)
             line_piece(chip, s, h, has_above, has_below, begin)
 
     def line_pieces(distance, s, act, wait):
@@ -444,13 +479,13 @@
             @pl.when(chip - distance >= 0)
             def _():
                 if wait:
-                    arrived(x, chip - distance, core, s, h)
+                    arrived(x, chip - distance, s, h)
                 line_piece(chip - distance, s, h, has_above, chip < 0, act)
 
             @pl.when(chip + distance < chips)
             def _():
                 if wait:
-                    arrived(x, chip + distance, core, s, h)
+                    arrived(x, chip + distance, s, h)
                 line_piece(chip + distance, s, h, chip < 0, has_below, act)
 
     def at_distance(distance, body):
@@ -469,13 +504,13 @@
     def cross(z, s, act, wait):
         for h in range(2):
             if wait:
-                arrived(1 - x, z, core, s, h)
-            act(piece_copy(1 - x, z, core, s, h, fan_send.at[1, z, s, h], partner))
+                arrived(1 - x, z, s, h)
+            act(fan_copy(1 - x, z, s, h))
 
     def a_copy(z, h):
         cols = columns(h, width)
         return remote(
-            sums.at[1 - core, z, :, :, cols], sums_in.at[z, :, :, cols], a_send.at[z, h],
+            sums.at[1 - core, z, :, :, cols], sums_in.at[z, :, :, cols], a_send.at[0],
             a_recv.at[z, h], partner,
         )
 
@@ -494,7 +529,8 @@
             ).astype(BF16)
 
     mix = Line(
-        chips, chip, sp, tp, lambda z, p: sums.at[core, z, p // 2, :, columns(p, width)],
+        chips, chip, sp, tp, lambda z: sums.at[core, z],
+        lambda z, p: sums.at[core, z, p // 2, :, columns(p, width)],
         a_down_in, a_up_in, a_sems,
     )
 
@@ -519,11 +555,11 @@
             line_piece(chip, y, h, has_above, has_below, begin)
 
     def p_copy(z):
-        return remote(part.at[z, 1 - core], partner_in.at[z], p_send.at[z], p_recv.at[z], partner)
+        return remote(part.at[z, 1 - core], partner_in.at[z], bulk.at[2], p_recv.at[z], partner)
 
     def xr_copy(z, s):
         return remote(
-            part.at[z, core, 1 - x, s], x_in.at[z, s], xr_send.at[z, s], xr_recv.at[z, s], x_peer
+            part.at[z, core, 1 - x, s], x_in.at[z, s], bulk.at[3], xr_recv.at[z, s], x_peer
         )
 
     lanes = lax.broadcasted_iota(jnp.int32, (1, router_ref.shape[0]), 1)
@@ -535,10 +571,8 @@
     expert_sign = signed(2 + sp, 2 + sp + 1 - 2 * x)
 
     def expert(z):
-        for h in range(2):
-            for xs in range(2):
-                for s in range(2):
-                    arrived(xs, z, 1 - core, s, h)
+        fanned = rows.at[:, z, 1 - core]
+        remote(fanned, fanned, bulk.at[0], fan_recv.at[z], partner).wait_recv()
         block = rows[:, z].reshape(8 * half_rows, width)
         logits = lax.dot_general(
             block, router_ref[...].astype(BF16), (((1,), (1,)), ((), ())), preferred_element_type=F32
@@ -673,9 +707,9 @@
 
     send_x(chip, y)
     back = Line(
-        chips, chip, sp, tp,
+        chips, chip, sp, tp, lambda z: part.at[z, core, x],
         lambda z, p: part.at[z, core, x, halves[p // 2], :, columns(p, width)],
-        down_in, up_in, (down_send, down_recv, up_send, up_recv),
+        down_in, up_in, a_sems,
     )
     def back_turn(distance, mine):
         back.send(
@@ -683,43 +717,59 @@
             range(PIECES), join_x,
         )
 
+    def end(copy):
+        copy.wait_send()
+
+    def drain_dispatch():
+        for h in range(2):
+            end(y_copy(h))
+        end(remote(sums.at[1 - core], sums_in, a_send.at[0], a_recv.at[0, 0], partner))
+        mine = rows.at[:, :, core]
+        end(remote(mine, mine, bulk.at[0], fan_recv.at[0], partner))
+        crossed = rows.at[x, :, core]
+        end(remote(crossed, crossed, bulk.at[1], fan_recv.at[0], x_peer))
+        for z in range(chips):
+            chunk = rows.at[x, z, core]
+
+            @pl.when((z >= chip) & has_below)
+            def _():
+                end(remote(chunk, chunk, line_send.at[z, 0], fan_recv.at[0], below))
+
+            @pl.when((z <= chip) & has_above)
+            def _():
+                end(remote(chunk, chunk, line_send.at[z, 1], fan_recv.at[0], above))
+
+        end(remote(part.at[:, 1 - core], partner_in, bulk.at[2], p_recv.at[0], partner))
+        drain_kv()
+
+    mix.drain()
     back_turn(1, is_end)
+    drain_dispatch()
     for distance in range(chips - 1, 1, -1):
         back_turn(distance, True)
     back_turn(1, jnp.logical_not(is_end))
     for p in range(PIECES):
         back.own(p, join_x)
         finished(p)
+    def out_copy(n):
+        cols = columns(n, width)
+        return pltpu.make_async_copy(out_buf.at[:, cols], out_ref.at[:, cols], out_sem.at[n])
+
     for n in range(2):
         cols = columns(n, width)
         back_copy(n).wait_recv()
         returned = lax.dot_general(
             sel_other, y_in[:, cols], (((0,), (0,)), ((), ())), preferred_element_type=F32
         )
-        out_ref[:, cols] = (total[:, cols] + returned).astype(BF16)
-
-    def end(copy):
-        copy.wait_send()
+        out_buf[:, cols] = (total[:, cols] + returned).astype(BF16)
+        out_copy(n).start()
 
     for n in range(2):
-        back_copy(n).wait_send()
-    for h in range(2):
-        y_copy(h).wait_send()
-        for s in range(2):
-            line_piece(chip, s, h, has_above, has_below, end)
-        for z in range(chips):
-            end(a_copy(z, h))
-    for s in range(2):
-        for distance in range(chips):
-            if distance:
-                line_pieces(distance, s, end, False)
-            at_distance(distance, lambda z: cross(z, s, end, False))
-    for z in range(chips):
-        end(p_copy(z))
-        for s in range(2):
-            end(xr_copy(z, s))
-    mix.drain()
+        end(back_copy(n))
+    end(remote(part.at[:, core, 1 - x], x_in, bulk.at[3], xr_recv.at[0, 0], x_peer))
     back.drain()
+    for n in range(2):
+        out_copy(n).wait()
 
 
 def layer_kernel(
@@ -750,17 +800,16 @@
     a_sems = scratch[mixer_count - 4 : mixer_count]
     w_copy = pltpu.make_async_copy(w_hbm, w_buf, w_sem)
     attended, drain_kv = attention(
-        sp_count, chips, heads, loads[:3], [w_copy, loads[3]] + weights,
+        sp_count, chips, heads, True, loads[:3], [w_copy, loads[3]] + weights,
         q_ref, k_ref, v_ref, off_ref, doc_ref,
         meta_ref, doc_col, k_buf, v_buf, m_buf, acc, carry, kv_send, kv_recv,
     )
     experts_kernel(
-        chips, weights, w_copy, loads[3], attended,
+        chips, weights, w_copy, loads[3], attended, drain_kv,
         mixed_ref, res_ref, gain_ref, ids_ref, group_ref, expert_ref, out_ref,
         w_buf, sums, sums_in, a_down_in, a_up_in, a_send, a_recv, a_sems,
         router_ref, gate, up, down, *scratch[mixer_count:],
     )
-    drain_kv()
 
 
 def pair_layer(
@@ -782,7 +831,7 @@
         ),
         out_shape=jax.ShapeDtypeStruct((rows, width), BF16),
         in_specs=[ANY_SPEC] * 8 + [VMEM_SPEC] * 6,
-        out_specs=VMEM_SPEC,
+        out_specs=ANY_SPEC,
         scratch_shapes=[
             pltpu.VMEM(queries.shape, BF16),
             pltpu.VMEM(keys.shape, BF16),
@@ -807,17 +856,16 @@
             pltpu.VMEM(quarter, BF16),
             pltpu.VMEM((half_rows, width), BF16),
             pltpu.VMEM((rows, width), F32),
+            pltpu.VMEM((rows, width), BF16),
+            dma((2,)),
             dma((7,)),
-            dma((2, chips, 2, 2, 2)),
-            dma((chips, 2, 2, 2)),
-            dma((chips, 2, 2)),
             dma((2, chips, 2, 2)),
             dma((chips,)),
+            dma((chips, 2)),
+            dma((4,)),
             dma((chips,)),
             dma((chips, 2)),
-            dma((chips, 2)),
-        ]
-        + [dma((chips, PIECES))] * 4,
+        ],
         compiler_params=pltpu.CompilerParams(
             collective_id=1, has_side_effects=True, vmem_limit_bytes=60 << 20
         ),

time: 103 us -> 101 us (0.981)
  Pallas kernels: 101 us -> 99.2 us
    pallas_call x1, Pallas kernels: 101 us -> 99.2 us  [pair_layer(): pl.pallas_call(functools.partial(layer_kernel, lax.axis_size('sp'), chips...]
where the time goes in v4:
time: 101 us
  Pallas kernels  99.2 us (98%)
  local copies, waits for them, and re-layouts  1.67 us (2%)
    pallas_call x1, Pallas kernels, pair_layer(): pl.pallas_call(functools.partial(layer_kernel, lax.axis_size('sp'), chips...  99.2 us

profile of v4, /device:TPU:0, one launch (start us, length us, event | category | flops | bytes accessed | tf_op | source)
XLA Modules:
  0.0 100.8 jit_solution(9027272430162632585)
XLA Ops:
  0.0 99.2 %layer.1 = bf16[32,4096]{1,0:T(8,128)(2,1)} custom-call(bf16[256,256]{1,0:T(8,128)(2,1)} %q_hbm.1, bf16[256,256]{1,0:T(8,128)(2,1)} %k_hbm.1, bf16[256,256]{1,0:T(8,128)(2,1)} %v_hbm.1, bf16[32,4096]{1,0:T(8,128)(2,1)} %res_hbm.1, bf16[256,4096]{1,0:T(8,128)(2,1)} %w_hbm.1, bf16[1,4096,512]{2,1,0:T(8,128)(2,1)} %gate_hbm.1, bf16[1,4096,512]{2,1,0:T(8,128)(2,1)} %up_hbm.1, ...), custom_call_target="tpu_custom_call" | custom-call | tf_op jit(solution)/shard_map/layer/pallas_call | solution.py:828
  99.2 1.7 %copy.16 = bf16[32,4096]{1,0:T(8,128)(2,1)} copy(bf16[32,4096]{1,0:T(8,128)(2,1)} %layer.1) | data formatting | bytes 524288

commit v5 on v4

--- a/solution.py
+++ b/solution.py
@@ -135,7 +135,7 @@
 
 
 def attention(
-    sp_count, chips, heads, relay, loads, later_loads,
+    sp_count, chips, heads, relay, tables, loads, later_loads,
     q_ref, k_ref, v_ref, off_ref, doc_ref,
     meta_ref, doc_col, k_buf, v_buf, m_buf, acc, carry, kv_send, kv_recv,
 ):
@@ -158,6 +158,8 @@
         greet((sp, tp + 2))
 
     expect = sp_count + jnp.where(chip > 0, 1, 0) + jnp.where(chip < chips - 1, 1, 0)
+    for copy in tables:
+        copy.wait()
     docs = doc_ref[...].astype(F32)
     meta_ref[...] = jnp.zeros_like(meta_ref)
     meta_ref[0:heads, :] = off_ref[...].astype(F32)
@@ -296,7 +298,7 @@
     half_rows = res_ref.shape[0] // 2
     w_copy = pltpu.make_async_copy(w_hbm, w_buf, w_sem)
     attended, drain_kv = attention(
-        sp_count, chips, heads, False, (), (w_copy,),
+        sp_count, chips, heads, False, (), (), (w_copy,),
         q_ref, k_ref, v_ref, off_ref, doc_ref,
         meta_ref, doc_col, k_buf, v_buf, m_buf, acc, carry, kv_send, kv_recv,
     )
@@ -775,8 +777,9 @@
 def layer_kernel(
     sp_count, chips, heads, mixer_count,
     q_hbm, k_hbm, v_hbm, res_hbm, w_hbm, gate_hbm, up_hbm, down_hbm,
-    off_ref, doc_ref, gain_ref, ids_ref, group_ref, expert_ref,
+    off_hbm, doc_hbm, gain_hbm, ids_hbm, group_hbm, expert_hbm,
     out_ref,
+    off_ref, doc_ref, gain_ref, ids_ref, group_ref, expert_ref, table_sem,
     q_ref, k_ref, v_ref, res_ref, mixed_ref, load_sem, weight_sem, router_ref,
     gate, up, down,
     *scratch,
@@ -791,7 +794,16 @@
         pltpu.make_async_copy(src.at[0], dst, weight_sem.at[n])
         for n, (src, dst) in enumerate(((gate_hbm, gate), (up_hbm, up), (down_hbm, down)))
     ]
-    for copy in loads[:3]:
+    tables = [
+        pltpu.make_async_copy(src, dst, table_sem.at[n])
+        for n, (src, dst) in enumerate(
+            (
+                (off_hbm, off_ref), (doc_hbm, doc_ref), (gain_hbm, gain_ref),
+                (ids_hbm, ids_ref), (group_hbm, group_ref), (expert_hbm, expert_ref),
+            )
+        )
+    ]
+    for copy in tables[:2] + loads[:3] + tables[2:]:
         copy.start()
     (
         meta_ref, doc_col, k_buf, v_buf, m_buf, acc, carry, w_buf, sums, sums_in, a_down_in, a_up_in,
@@ -800,7 +812,7 @@
     a_sems = scratch[mixer_count - 4 : mixer_count]
     w_copy = pltpu.make_async_copy(w_hbm, w_buf, w_sem)
     attended, drain_kv = attention(
-        sp_count, chips, heads, True, loads[:3], [w_copy, loads[3]] + weights,
+        sp_count, chips, heads, True, tables, loads[:3], [w_copy, loads[3]] + weights,
         q_ref, k_ref, v_ref, off_ref, doc_ref,
         meta_ref, doc_col, k_buf, v_buf, m_buf, acc, carry, kv_send, kv_recv,
     )
@@ -821,6 +833,9 @@
     heads = offsets.shape[1]
     mixer_parts = mixer_scratch(residual, queries, heads, out_weight)
     half_rows = rows // 2
+    tables = (
+        offsets.T, docs[None, :], gain[None, :], expert_ids.T, group_router.T, expert_router.T,
+    )
     units = gate.shape[2]
     half = (chips, 2, half_rows, width)
     quarter = (chips, PIECES, half_rows, width // 2)
@@ -830,9 +845,11 @@
             layer_kernel, lax.axis_size("sp"), chips, heads, len(mixer_parts)
         ),
         out_shape=jax.ShapeDtypeStruct((rows, width), BF16),
-        in_specs=[ANY_SPEC] * 8 + [VMEM_SPEC] * 6,
+        in_specs=[ANY_SPEC] * 14,
         out_specs=ANY_SPEC,
-        scratch_shapes=[
+        scratch_shapes=[pltpu.VMEM(table.shape, table.dtype) for table in tables]
+        + [
+            dma((len(tables),)),
             pltpu.VMEM(queries.shape, BF16),
             pltpu.VMEM(keys.shape, BF16),
             pltpu.VMEM(values.shape, BF16),
@@ -872,7 +889,7 @@
         name="layer",
     )(
         queries, keys, values, residual, out_weight, gate, up, down,
-        offsets.T, docs[None, :], gain[None, :], expert_ids.T, group_router.T, expert_router.T,
+        *tables,
     )
 
 

time: 101 us -> 100 us (0.990)
  no operation moved by 1% of the time
where the time goes in v5:
time: 100 us
  Pallas kernels  98.4 us (98%)
  local copies, waits for them, and re-layouts  1.67 us (2%)
    pallas_call x1, Pallas kernels, pair_layer(): pl.pallas_call(functools.partial(layer_kernel, lax.axis_size('sp'), chips...  98.4 us

profile of v5, /device:TPU:0, one launch (start us, length us, event | category | flops | bytes accessed | tf_op | source)
XLA Modules:
  0.0 100.1 jit_solution(12547998594978977684)
XLA Ops:
  0.0 98.4 %layer.1 = bf16[32,4096]{1,0:T(8,128)(2,1)} custom-call(bf16[256,256]{1,0:T(8,128)(2,1)} %q_hbm.1, bf16[256,256]{1,0:T(8,128)(2,1)} %k_hbm.1, bf16[256,256]{1,0:T(8,128)(2,1)} %v_hbm.1, bf16[32,4096]{1,0:T(8,128)(2,1)} %res_hbm.1, bf16[256,4096]{1,0:T(8,128)(2,1)} %w_hbm.1, bf16[1,4096,512]{2,1,0:T(8,128)(2,1)} %gate_hbm.1, bf16[1,4096,512]{2,1,0:T(8,128)(2,1)} %up_hbm.1, ...), custom_call_target="tpu_custom_call" | custom-call | tf_op jit(solution)/shard_map/layer/pallas_call | solution.py:843
  98.4 1.7 %copy.16 = bf16[32,4096]{1,0:T(8,128)(2,1)} copy(bf16[32,4096]{1,0:T(8,128)(2,1)} %layer.1) | data formatting | bytes 524288
